TPU v7x, 128 devices: a whole 4x4x4 slice. The times are simulated.
128 devices in a mesh: sp: 64 (over z, y, x), tp: 2 (over core).
Axes of the slice: x: 4, y: 4, z: 4, core: 2. Of those that a mesh axis runs over, the one named last changes fastest.
Arguments:
- residual: bfloat16 [16384, 2048], P(('sp', 'tp')), may hold values from -6 to 6
- pool_input: bfloat16 [16384, 1024], P('sp', 'tp'), may hold values from -6 to 6
- group_maps: bfloat16 [8, 128, 128], replicated, may hold values from -0.5 to 0.5
- pool_scale: float32 [1024], replicated, may hold values from 0.1 to 1.9
- out_proj: bfloat16 [1024, 2048], replicated, may hold values from -0.1875 to 0.1875
- norm_gain: float32 [2048], replicated, may hold values from 0.1 to 1.9
- shared_gate: bfloat16 [2048, 512], replicated, may hold values from -0.125 to 0.125
- shared_up: bfloat16 [2048, 512], replicated, may hold values from -0.125 to 0.125
- shared_down: bfloat16 [512, 2048], replicated, may hold values from -0.25 to 0.25
- expert_gate: bfloat16 [128, 2048, 512], P(('sp', 'tp')), may hold values from -0.125 to 0.125
- expert_up: bfloat16 [128, 2048, 512], P(('sp', 'tp')), may hold values from -0.125 to 0.125
- expert_down: bfloat16 [128, 512, 2048], P(('sp', 'tp')), may hold values from -0.25 to 0.25
- expert_ids: int32 [16384, 4], P(('sp', 'tp')), may hold values from 0 to 127, all different within a row; in each aligned block of 128 rows (0 to 127, 128 to 255, ...) at most 6 rows name the same one
- route_score: float32 [16384, 4], P(('sp', 'tp')), may hold values from 0.05 to 1
Outputs:
- output: bfloat16 [16384, 2048], P(('sp', 'tp'))
Inputs may be any that keep to these rules, and one draw needn't show every extreme that they name: `expert_ids`: each row names 4 different experts; among the 128 rows of one device no expert is named more than 6 times, and in some devices' rows one expert is named exactly 6 times.
All inputs are finite; a program needn't handle non-finite values.
Results may differ from a plain program's by a relative error of at most 0.015.
Values may be sent and summed in bfloat16 or wider, within the bound.
A program may use at most 128 MiB of HBM per device.

v0:
```python
import jax
import jax.numpy as jnp
from jax import lax
from jax.sharding import PartitionSpec as P

windows = (2, 4, 8, 16)
epsilon = 1e-06
routed_scale = 2.5


def from_behind(shard, axis, by):
    peers = lax.axis_size(axis)
    pairs = [(i, i + by) for i in range(peers) if 0 <= i + by < peers]
    return lax.ppermute(shard, axis, pairs)


def swiglu(row_block, w_gate, w_up, w_down):
    gate_part = jnp.dot(row_block, w_gate, preferred_element_type=jnp.float32)
    up_part = jnp.dot(row_block, w_up, preferred_element_type=jnp.float32)
    hidden = (jax.nn.silu(gate_part) * up_part).astype(jnp.bfloat16)
    return jnp.dot(hidden, w_down, preferred_element_type=jnp.float32)


def on_device(
    residual,
    pool_input,
    group_maps,
    pool_scale,
    out_proj,
    norm_gain,
    shared_gate,
    shared_up,
    shared_down,
    expert_gate,
    expert_up,
    expert_down,
    expert_ids,
    route_score,
):
    row_count, channels = pool_input.shape
    group_width = group_maps.shape[1]
    groups_here = channels // group_width
    halo_reach = max(windows) - 1
    before = from_behind(pool_input[row_count - halo_reach :], "sp", 1)
    extended = (
        jnp.concatenate([before, pool_input], axis=0)
        .astype(jnp.float32)
        .reshape(row_count + halo_reach, groups_here, group_width)
    )
    places = lax.axis_index("sp") * row_count + jnp.arange(row_count, dtype=jnp.int32)
    pooled = []
    for group_index in range(groups_here):
        running_sum = extended[:, group_index]
        window_span = 1
        while window_span < windows[group_index % 4]:
            running_sum = running_sum[window_span:] + running_sum[:-window_span]
            window_span = window_span * 2
        divisor = jnp.minimum(places + 1, window_span).astype(jnp.float32)[:, None]
        pooled.append(running_sum[running_sum.shape[0] - row_count :] / divisor)
    pooled = jnp.stack(pooled, axis=1)
    contrast = (pooled - extended[halo_reach:]).astype(jnp.bfloat16)
    first_group = lax.axis_index("tp") * groups_here
    maps_here = lax.dynamic_slice_in_dim(group_maps, first_group, groups_here, 0)
    mapped = jnp.einsum("sgc,gcd->sgd", contrast, maps_here, preferred_element_type=jnp.float32)
    scale_here = lax.dynamic_slice_in_dim(pool_scale, first_group * group_width, channels, 0)
    mixed_rows = (mapped.reshape(row_count, channels) * scale_here).astype(jnp.bfloat16)
    model_width = out_proj.shape[1]
    swapped = lax.all_to_all(mixed_rows, "tp", split_axis=0, concat_axis=1, tiled=True)
    projected = jnp.dot(swapped, out_proj, preferred_element_type=jnp.float32)
    settled = (residual.astype(jnp.float32) + projected).astype(jnp.bfloat16)
    settled_wide = settled.astype(jnp.float32)
    inverse_rms = lax.rsqrt(jnp.mean(settled_wide * settled_wide, axis=-1, keepdims=True) + epsilon)
    normed = (settled_wide * inverse_rms * norm_gain).astype(jnp.bfloat16)
    shared = swiglu(normed, shared_gate, shared_up, shared_down)
    tokens_here, top_count = expert_ids.shape
    size_sp = lax.axis_size("sp")
    size_tp = lax.axis_size("tp")
    experts = size_sp * size_tp
    capacity = 3 * tokens_here * top_count // (2 * experts)
    assigned = tokens_here * top_count
    flat_ids = expert_ids.reshape(assigned)
    onehot = (flat_ids[:, None] == jnp.arange(experts, dtype=jnp.int32)[None, :]).astype(
        jnp.bfloat16
    )
    earlier = (jnp.arange(assigned)[None, :] < jnp.arange(assigned)[:, None]).astype(jnp.bfloat16)
    before_counts = jnp.dot(earlier, onehot, preferred_element_type=jnp.float32)
    position = jnp.sum(before_counts * onehot, axis=1).astype(jnp.int32)
    slot_index = position * experts + flat_ids
    slot_token = (
        jnp.zeros((capacity * experts,), jnp.int32)
        .at[slot_index]
        .set(jnp.arange(assigned, dtype=jnp.int32) // top_count)
    )
    outgoing = normed[slot_token].reshape(capacity, experts, model_width)
    arrived = lax.all_to_all(outgoing, ("sp", "tp"), split_axis=1, concat_axis=1, tiled=True)
    item_total = arrived.shape[0]
    flat_rows = arrived.reshape(item_total * experts, model_width)
    expert_rows = swiglu(flat_rows, expert_gate[0], expert_up[0], expert_down[0]).astype(
        jnp.bfloat16
    )
    results = expert_rows.reshape(item_total, experts, model_width)
    returned = lax.all_to_all(results, ("sp", "tp"), split_axis=1, concat_axis=1, tiled=True)
    picked = returned.reshape(capacity * experts, model_width)[slot_index].reshape(
        tokens_here, top_count, model_width
    )
    weights = route_score / jnp.sum(route_score, axis=-1, keepdims=True) * routed_scale
    routed = jnp.einsum("tk,tkd->td", weights, picked.astype(jnp.float32))
    return (settled_wide + shared + routed).astype(jnp.bfloat16)


def solution(mesh):
    in_specs = (
        P(("sp", "tp"), None),
        P("sp", "tp"),
        P(),
        P(),
        P(),
        P(),
        P(),
        P(),
        P(),
        P(("sp", "tp"), None, None),
        P(("sp", "tp"), None, None),
        P(("sp", "tp"), None, None),
        P(("sp", "tp"), None),
        P(("sp", "tp"), None),
    )
    out_specs = P(("sp", "tp"), None)
    return jax.shard_map(
        on_device, mesh=mesh, in_specs=in_specs, out_specs=out_specs, check_vma=False
    )
```

profile of v0, /device:TPU:1, one launch (start us, length us, event | category | flops | bytes accessed | tf_op | source)
XLA Modules:
  0.0 196.1 jit_solution(7039862914331107756)
XLA Ops:
  0.0 0.0 copy-start
  0.0 0.9 slice.118
  0.9 3.9 %collective-permute-start = (bf16[15,512]{1,0:T(8,128)(2,1)S(1)}, bf16[15,512]{1,0:T(8,128)(2,1)S(1)}, u32[]{:S(2)}, u32[]{:S(2)}) collective-permute-start(bf16[15,512]{1,0:T(8,128)(2,1)S(1)} %slice.118), channel_id=1, source_target_pairs={{0,2},{2,4},{4,6},{6,8},{8,10},{10,12},{12,14},{14,16},{16,18},{18... | collective-permute-start | bytes 46088 | tf_op jit(solution)/shard_map/ppermute | solution.py:14
  4.8 1.0 copy_bitcast_fusion
  5.8 0.8 copy.41
  6.6 0.1 eq.15
  6.7 0.1 reshape.132
  6.8 0.3 fusion.12
  7.2 2.4 %scatter_custom_fusion = s32[768]{0:T(1024)S(1)} fusion(s32[512]{0:T(512)S(1)} %bitcast.90, s32[512]{0:T(512)S(1)} %add_select_fusion, s32[]{:T(128)} %constant.22.clone.1), kind=kCustom, calls=%fused_computation.73 | custom fusion | bytes 3076 | tf_op jit(solution)/shard_map/scatter | solution.py:92
  9.7 0.8 dynamic_slice.7
  10.5 0.0 collective-permute-done
  10.5 0.1 maximum_convert_fusion
  10.6 0.1 fusion.48
  10.6 0.0 copy-start.3
  10.6 0.0 copy-start.4
  10.8 0.1 fusion.26
  10.9 0.1 fusion.29
  11.0 0.1 fusion.32
  11.1 0.1 fusion.35
  11.2 0.3 copy-done.3
  11.6 0.1 copy-done.4
  11.7 0.3 convolution_bitcast_fusion
  11.9 0.3 reshape.131
  12.2 0.1 fusion.16
  12.4 4.5 %all_to_all.26 = bf16[2,128,512]{1,2,0:T(8,128)(2,1)S(1)} all-to-all(bf16[2,128,512]{1,2,0:T(8,128)(2,1)S(1)} %fusion.16), channel_id=1, replica_groups=mesh['sp'=64,'tp'=2] {'tp'}, dimensions={0} | all-to-all | bytes 524288 | tf_op jit(solution)/shard_map/all_to_all | solution.py:68
  16.9 0.0 copy-start.5
  16.9 3.1 %multiply_reduce_fusion = (f32[128]{0:T(128)S(1)}, f32[128,2048]{1,0:T(8,128)S(1)}) fusion(bf16[128,1024]{0,1:T(8,128)(2,1)S(1)} %bitcast.89, bf16[1024,2048]{1,0:T(8,128)(2,1)} %param.18, bf16[128,2048]{1,0:T(8,128)(2,1)} %param.14), kind=kOutput, calls=%fused_computation.23 | convolution fusion | flops 538443648 | bytes 6029824 | tf_op jit(solution)/shard_map/dot_general | solution.py:69
  20.0 0.0 copy-start.1
  20.1 1.0 copy-done.1
  21.1 0.0 copy-done.5
  21.1 0.2 multiply_convert_fusion.1
  21.2 4.2 %gather_fusion = bf16[768,2048]{1,0:T(8,128)(2,1)} fusion(bf16[128,2048]{1,0:T(8,128)(2,1)S(1)} %multiply_convert_fusion.1, s32[1024]{0:T(1024)S(1)} %pad_clamp_fusion.1), kind=kCustom, calls=%fused_computation | custom fusion | bytes 6294528 | tf_op jit(solution)/shard_map/gather | solution.py:94
  25.5 3.6 %copy.43 = bf16[6,128,2048]{2,0,1:T(8,128)(2,1)S(1)} copy(bf16[6,128,2048]{2,1,0:T(8,128)(2,1)} %bitcast.85) | data formatting | bytes 6291456 | tf_op jit(solution)/shard_map/reshape | solution.py:94
  29.1 62.8 %all_to_all.27 = bf16[6,128,2048]{2,0,1:T(8,128)(2,1)S(1)} all-to-all(bf16[6,128,2048]{2,0,1:T(8,128)(2,1)S(1)} %copy.43), channel_id=1, replica_groups=mesh['sp'=64,'tp'=2] {'sp','tp'}, dimensions={1} | all-to-all | bytes 6291456 | tf_op jit(solution)/shard_map/all_to_all | solution.py:95
  92.0 0.0 copy-start.7
  92.0 1.7 copy.44
  93.7 0.0 copy-start.2
  93.7 1.7 copy-done.2
  95.4 0.0 copy-done.7
  95.4 2.9 %fusion.7 = f32[768,512]{1,0:T(8,128)} fusion(bf16[768,2048]{1,0:T(8,128)(2,1)S(1)} %bitcast.86, bf16[1,2048,512]{2,1,0:T(8,128)(2,1)S(1)} %copy-done.7), kind=kOutput, calls=%fused_computation.13 | convolution fusion | flops 1610612736 | bytes 6815744 | tf_op jit(solution)/shard_map/dot_general | solution.py:18
  98.3 0.0 copy-done
  98.3 8.1 %convolution_convert_fusion = bf16[768,2048]{1,0:T(8,128)(2,1)} fusion(bf16[1,512,2048]{2,1,0:T(8,128)(2,1)S(1)} %copy-done, f32[768,512]{1,0:T(8,128)} %fusion.7, bf16[768,2048]{1,0:T(8,128)(2,1)} %bitcast.87, bf16[1,2048,512]{2,1,0:T(8,128)(2,1)} %param.24), kind=kOutput, calls=%fused_computation.3 | convolution fusion | flops 3225157632 | bytes 12058624 | tf_op jit(solution)/shard_map/dot_general | solution.py:21
  106.4 5.6 %copy.45 = bf16[6,128,2048]{2,0,1:T(8,128)(2,1)} copy(bf16[6,128,2048]{2,1,0:T(8,128)(2,1)} %bitcast.88) | data formatting | bytes 6291456 | tf_op jit(solution)/shard_map/reshape | solution.py:101
  112.0 0.0 copy-start.6
  112.0 5.6 %all-to-all-start.2 = ((bf16[6,128,2048]{2,0,1:T(8,128)(2,1)}), bf16[6,128,2048]{2,0,1:T(8,128)(2,1)}, u32[]{:S(2)}, u32[]{:S(2)}) async-start(bf16[6,128,2048]{2,0,1:T(8,128)(2,1)} %copy.45), calls=%async_computation.2 | async-start | bytes 8388608 | tf_op jit(solution)/shard_map/all_to_all | solution.py:102
  117.7 0.0 copy-done.6
  117.7 0.1 copy.47
  117.9 2.0 %fusion.51 = f32[128,512]{1,0:T(8,128)S(1)} fusion(bf16[128,2048]{1,0:T(8,128)(2,1)S(1)} %multiply_convert_fusion.1, bf16[2048,512]{1,0:T(8,128)(2,1)} %param.20), kind=kOutput, calls=%fused_computation.90 | convolution fusion | flops 268435456 | bytes 2883584 | tf_op jit(solution)/shard_map/dot_general | solution.py:18
  119.9 50.5 %all-to-all-done.2 = bf16[6,128,2048]{2,0,1:T(8,128)(2,1)} async-done(((bf16[6,128,2048]{2,0,1:T(8,128)(2,1)}), bf16[6,128,2048]{2,0,1:T(8,128)(2,1)}, u32[]{:S(2)}, u32[]{:S(2)}) %all-to-all-start.2) | async-done | bytes 3145760 | tf_op jit(solution)/shard_map/all_to_all | solution.py:102
  170.4 5.6 %copy.46 = bf16[6,128,2048]{2,1,0:T(8,128)(2,1)} copy(bf16[6,128,2048]{2,0,1:T(8,128)(2,1)} %all-to-all-done.2) | data formatting | bytes 6291456 | tf_op jit(solution)/shard_map/all_to_all | solution.py:102
  176.0 7.6 %gather_fusion.1 = bf16[512,2048]{1,0:T(8,128)(2,1)} fusion(bf16[768,2048]{1,0:T(8,128)(2,1)} %bitcast.84, s32[1024]{0:T(1024)S(1)} %pad_clamp_fusion), kind=kCustom, calls=%fused_computation.1 | custom fusion | bytes 4196352 | tf_op jit(solution)/shard_map/gather | solution.py:103
  183.6 4.1 %reshape.137 = bf16[128,4,2048]{2,1,0:T(4,128)(2,1)} reshape(bf16[512,2048]{1,0:T(8,128)(2,1)} %gather_fusion.1) | data formatting | bytes 4194304 | tf_op jit(solution)/shard_map/reshape | solution.py:103
  187.7 3.8 %fusion.52 = f32[128,1,2048]{2,1,0:T(1,128)} fusion(bf16[128,4,1]{1,2,0:T(2,128)(2,1)S(1)} %copy.47, bf16[128,4,2048]{2,1,0:T(4,128)(2,1)} %reshape.137), kind=kOutput, calls=%fused_computation.91 | convolution fusion | flops 2097152 | bytes 3146752 | tf_op jit(solution)/shard_map/tk,tkd->td/dot_general | solution.py:107
  191.4 4.7 %fusion.3 = bf16[128,2048]{1,0:T(8,128)(2,1)} fusion(f32[128,2048]{1,0:T(8,128)} %copy-done.1, bf16[512,2048]{1,0:T(8,128)(2,1)} %param.22, bf16[128,2048]{1,0:T(8,128)(2,1)S(1)} %multiply_convert_fusion.1, bf16[2048,512]{1,0:T(8,128)(2,1)} %param.21, f32[128,1,2048]{2,1,0:T(1,128)} %fusion.52, f32[128,512]{1,0:T(8,128)S(1)} %fusion.51), kind=kOutput, calls=%fused_computation.9 | convolution fusion | flops 538050560 | bytes 7602176 | tf_op jit(solution)/shard_map/dot_general | solution.py:21
  (17 shorter events, 0.2 us)
Async XLA Ops:
  0.0 98.3 %copy-start = (bf16[1,512,2048]{2,1,0:T(8,128)(2,1)S(1)}, bf16[1,512,2048]{2,1,0:T(8,128)(2,1)}, u32[]{:S(2)}) copy-start(bf16[1,512,2048]{2,1,0:T(8,128)(2,1)} %param.25) | copy-start | bytes 6291460
  0.9 9.6 %collective-permute-start = (bf16[15,512]{1,0:T(8,128)(2,1)S(1)}, bf16[15,512]{1,0:T(8,128)(2,1)S(1)}, u32[]{:S(2)}, u32[]{:S(2)}) collective-permute-start(bf16[15,512]{1,0:T(8,128)(2,1)S(1)} %slice.118), channel_id=1, source_target_pairs={{0,2},{2,4},{4,6},{6,8},{8,10},{10,12},{12,14},{14,16},{16,18},{18... | collective-permute-start | bytes 46088 | tf_op jit(solution)/shard_map/ppermute | solution.py:14
  10.6 1.0 copy-start.3
  10.6 1.0 copy-start.4
  16.9 4.2 %copy-start.5 = (f32[2048]{0:T(1024)S(1)}, f32[2048]{0:T(1024)}, u32[]{:S(2)}) copy-start(f32[2048]{0:T(1024)} %param.19) | copy-start | bytes 24580
  20.0 1.1 copy-start.1
  92.0 3.4 %copy-start.7 = (bf16[1,2048,512]{2,1,0:T(8,128)(2,1)S(1)}, bf16[1,2048,512]{2,1,0:T(8,128)(2,1)}, u32[]{:S(2)}) copy-start(bf16[1,2048,512]{2,1,0:T(8,128)(2,1)} %param.23) | copy-start | bytes 6291460
  93.7 1.7 copy-start.2
  112.0 5.7 %copy-start.6 = (f32[128,4]{0,1:T(4,128)S(1)}, f32[128,4]{0,1:T(4,128)}, u32[]{:S(2)}) copy-start(f32[128,4]{0,1:T(4,128)} %param.27) | copy-start | bytes 6148
  112.0 58.4 %all-to-all-start.2 = ((bf16[6,128,2048]{2,0,1:T(8,128)(2,1)}), bf16[6,128,2048]{2,0,1:T(8,128)(2,1)}, u32[]{:S(2)}, u32[]{:S(2)}) async-start(bf16[6,128,2048]{2,0,1:T(8,128)(2,1)} %copy.45), calls=%async_computation.2 | async-start | bytes 8388608 | tf_op jit(solution)/shard_map/all_to_all | solution.py:102
where the time goes:
time: 197 us; the launch traced here: 196 us
  blocking collectives  67.3 us (34%)
  waiting for transfers between devices  50.5 us (26%)
  local copies, waits for them, and re-layouts  42.2 us (21%)
  matrix products  25.3 us (13%)
  starting transfers between devices  9.56 us (5%)
    all_to_all x1, blocking collectives, on_device(): lax.all_to_all(outgoing, ('sp', 'tp'), split_axis=1, concat_axis=1, tiled...  62.8 us
    all_to_all x1, waiting for transfers between devices, on_device(): lax.all_to_all(results, ('sp', 'tp'), split_axis=1, concat_axis=1, tiled=...  50.5 us
    dot_general x2, matrix products, swiglu(): return jnp.dot(hidden, w_down, preferred_element_type=jnp.float32)  12.8 us
    gather x1, local copies, waits for them, and re-layouts, on_device(): returned.reshape(capacity * experts, model_width)[slot_index]  7.58 us
    all_to_all x1, starting transfers between devices, on_device(): lax.all_to_all(results, ('sp', 'tp'), split_axis=1, concat_axis=1, tiled=...  5.64 us
    reshape x1, local copies, waits for them, and re-layouts, on_device(): results = expert_rows.reshape(item_total, experts, model_width)  5.63 us
    all_to_all x1, local copies, waits for them, and re-layouts, on_device(): lax.all_to_all(results, ('sp', 'tp'), split_axis=1, concat_axis=1, tiled=...  5.59 us
    dot_general x2, matrix products, swiglu(): gate_part = jnp.dot(row_block, w_gate, preferred_element_type=jnp.float32)  4.97 us
  transfers between devices with their start and end apart: 2, of which 1 were waited for; matrix products, arithmetic and copies ran while one was open for 4% of the time, Pallas kernels for 0%

commit v1 on v0

v1 whole, which is shorter than its diff:
```python
import functools

import jax
import jax.numpy as jnp
from jax import lax
from jax.experimental import pallas as pl
from jax.experimental.pallas import tpu as pltpu
from jax.sharding import PartitionSpec as P

windows = (2, 4, 8, 16)
epsilon = 1e-06
routed_scale = 2.5

MESH = pl.DeviceIdType.MESH
F32 = jnp.float32
BF16 = jnp.bfloat16

SIDE = 4
DEVICES = 128
TOKENS_HERE = 128
TOPK = 4
CAP = 6
SLOTS = 8
D = 2048
HID = 512
ROWS = 256
CHANNELS = 512
GROUPS = 4
GW = 128
REACH = 16
STRIDE = 53
PARTS = 4
PEERS = DEVICES // PARTS


def dot(a, b):
    return jnp.dot(a, b, preferred_element_type=F32)


def offset_of(k):
    kk = lax.rem(k * STRIDE, DEVICES)
    c = lax.rem(kk, 2)
    x = lax.rem(lax.div(kk, 2), SIDE)
    y = lax.rem(lax.div(kk, 8), SIDE)
    z = lax.div(kk, 32)
    return z, y, x, c


def shifted(sp, tp, k, sign):
    dz, dy, dx, dc = offset_of(k)
    z = lax.div(sp, SIDE * SIDE)
    y = lax.rem(lax.div(sp, SIDE), SIDE)
    x = lax.rem(sp, SIDE)
    z = lax.rem(z + sign * dz + SIDE, SIDE)
    y = lax.rem(y + sign * dy + SIDE, SIDE)
    x = lax.rem(x + sign * dx + SIDE, SIDE)
    c = lax.rem(tp + dc, 2)
    return (z * SIDE + y) * SIDE + x, c


def kernel(
    res_hbm, pool_hbm, maps_hbm, scale_hbm, proj_hbm, gain_hbm,
    sg_hbm, su_hbm, sd_hbm, eg_hbm, eu_hbm, ed_hbm, ids_hbm, score_hbm,
    out_ref,
    res, ext, maps, scale, proj, gain, sg, su, sd, eg, eu, ed, ids, score,
    mix, halves, settled, normed, acc, place, comb,
    outgoing, arrived, results, returned,
    in_sems, halo_send, halo_recv, swap_send, swap_recv,
    out_send, out_recv, back_send, back_recv,
):
    sp = lax.axis_index("sp")
    tp = lax.axis_index("tp")

    def fetch(i, src, dst):
        copy = pltpu.make_async_copy(src, dst, in_sems.at[i])
        copy.start()
        return copy

    get_pool = fetch(0, pool_hbm, ext.at[pl.ds(REACH, ROWS)])
    get_ids = fetch(1, ids_hbm, ids)
    get_score = fetch(2, score_hbm, score)
    get_maps = fetch(3, maps_hbm.at[pl.ds(tp * GROUPS, GROUPS)], maps)
    get_scale = fetch(4, scale_hbm, scale)
    get_res = fetch(5, res_hbm, res)
    get_gain = fetch(6, gain_hbm, gain)
    get_proj = fetch(7, proj_hbm, proj)
    get_sg = fetch(8, sg_hbm, sg)
    get_su = fetch(9, su_hbm, su)
    get_sd = fetch(10, sd_hbm, sd)
    get_eg = fetch(11, eg_hbm.at[0], eg)
    get_eu = fetch(12, eu_hbm.at[0], eu)
    get_ed = fetch(13, ed_hbm.at[0], ed)

    def clear(i, _):
        returned[pl.ds(i * 8, 8)] = jnp.zeros((8, SLOTS, D), BF16)
        return 0

    lax.fori_loop(0, DEVICES // 8, clear, 0)

    barrier = pltpu.get_barrier_semaphore()

    def greet(k, _):
        pl.semaphore_signal(barrier, inc=1, device_id=shifted(sp, tp, k, 1), device_id_type=MESH)
        return 0

    lax.fori_loop(1, DEVICES, greet, 0)
    get_pool.wait()
    pl.semaphore_wait(barrier, DEVICES - 1)

    halo = pltpu.make_async_remote_copy(
        ext.at[pl.ds(ROWS, REACH)], ext.at[pl.ds(0, REACH)], halo_send, halo_recv,
        device_id=(lax.rem(sp + 1, DEVICES // 2), tp), device_id_type=MESH,
    )
    halo.start()

    get_ids.wait()
    get_score.wait()
    expert = lax.broadcasted_iota(jnp.int32, (DEVICES, TOKENS_HERE), 0)
    raw = score[...]
    weights = raw / jnp.sum(raw, axis=0, keepdims=True) * routed_scale
    chosen = jnp.zeros((DEVICES, TOKENS_HERE), F32)
    weight = jnp.zeros((DEVICES, TOKENS_HERE), F32)
    for k in range(TOPK):
        hit = expert == ids[k : k + 1, :]
        chosen = jnp.where(hit, 1.0, chosen)
        weight = jnp.where(hit, weights[k : k + 1, :], weight)
    row = lax.broadcasted_iota(jnp.int32, (TOKENS_HERE, TOKENS_HERE), 0)
    column = lax.broadcasted_iota(jnp.int32, (TOKENS_HERE, TOKENS_HERE), 1)
    earlier = (row < column).astype(BF16)
    rank = dot(chosen.astype(BF16), earlier)
    tag = chosen * (rank + 1.0)
    slot_row = lax.broadcasted_iota(jnp.int32, (DEVICES * SLOTS, DEVICES), 0)
    slot_expert = lax.broadcasted_iota(jnp.int32, (DEVICES * SLOTS, DEVICES), 1)
    peer_sp, peer_tp = shifted(sp, tp, lax.div(slot_row, SLOTS), 1)
    spread = (peer_sp * 2 + peer_tp == slot_expert).astype(BF16)
    slot_number = (lax.rem(slot_row, SLOTS) + 1).astype(F32)
    place[...] = (dot(spread, tag.astype(BF16)) == slot_number).astype(BF16)
    weight_high = weight.astype(BF16)
    weight_low = (weight - weight_high.astype(F32)).astype(BF16)
    comb[:, :TOKENS_HERE] = dot(spread, weight_high).astype(BF16) * place[...]
    comb[:, TOKENS_HERE:] = dot(spread, weight_low).astype(BF16) * place[...]

    get_maps.wait()
    get_scale.wait()
    halo.wait()
    center = lax.broadcasted_iota(jnp.int32, (ROWS, REACH + ROWS), 0) + REACH
    other = lax.broadcasted_iota(jnp.int32, (ROWS, REACH + ROWS), 1)
    real = (other >= REACH) | (sp > 0)
    position = sp * ROWS + lax.broadcasted_iota(jnp.int32, (ROWS, GW), 0)
    for g in range(GROUPS):
        lanes = slice(g * GW, (g + 1) * GW)
        band = (other <= center) & (other > center - windows[g]) & real
        total = dot(band.astype(BF16), ext[:, lanes])
        divisor = jnp.minimum(position + 1, windows[g]).astype(F32)
        contrast = (total / divisor - ext[REACH:, lanes].astype(F32)).astype(BF16)
        mapped = dot(contrast, maps[g])
        row_scale = jnp.where(tp == 0, scale[g : g + 1, :], scale[GROUPS + g : GROUPS + g + 1, :])
        mix[:, lanes] = (mapped * row_scale).astype(BF16)

    swap = pltpu.make_async_remote_copy(
        mix.at[pl.ds(pl.multiple_of((1 - tp) * TOKENS_HERE, TOKENS_HERE), TOKENS_HERE)],
        halves, swap_send, swap_recv, device_id=(sp, 1 - tp), device_id_type=MESH,
    )
    swap.start()

    get_res.wait()
    get_gain.wait()
    get_proj.wait()
    own = mix[pl.ds(pl.multiple_of(tp * TOKENS_HERE, TOKENS_HERE), TOKENS_HERE), :]
    for n in range(0, D, 512):
        near = proj[pl.ds(pl.multiple_of(tp * CHANNELS, CHANNELS), CHANNELS), n : n + 512]
        acc[:, n : n + 512] = dot(own, near)
    swap.wait()
    square = jnp.zeros((TOKENS_HERE, 1), F32)
    for n in range(0, D, 512):
        far = proj[pl.ds(pl.multiple_of((1 - tp) * CHANNELS, CHANNELS), CHANNELS), n : n + 512]
        value = acc[:, n : n + 512] + dot(halves[...], far)
        value = (value + res[:, n : n + 512].astype(F32)).astype(BF16)
        settled[:, n : n + 512] = value
        value = value.astype(F32)
        square = square + jnp.sum(value * value, axis=1, keepdims=True)
    inverse = lax.rsqrt(square / D + epsilon)
    for j in range(D // 128):
        lanes = slice(j * 128, (j + 1) * 128)
        value = settled[:, lanes].astype(F32) * inverse * gain[j : j + 1, :]
        normed[:, lanes] = value.astype(BF16)

    def fill(i, _):
        n = pl.multiple_of(i * 256, 256)
        rows = dot(place[...], normed[:, pl.ds(n, 256)]).astype(BF16)
        outgoing[:, :, pl.ds(n, 256)] = rows.reshape(DEVICES, SLOTS, 256)
        return 0

    lax.fori_loop(0, D // 256, fill, 0)

    def send(k, part):
        pltpu.make_async_remote_copy(
            outgoing.at[k, pl.ds(0, CAP)], arrived.at[k, pl.ds(0, CAP)],
            out_send, out_recv.at[part],
            device_id=shifted(sp, tp, k, 1), device_id_type=MESH,
        ).start()
        return part

    def send_back(k, part):
        pltpu.make_async_remote_copy(
            results.at[k, pl.ds(0, CAP)], returned.at[k, pl.ds(0, CAP)],
            back_send, back_recv.at[part],
            device_id=shifted(sp, tp, k, -1), device_id_type=MESH,
        ).start()
        return part

    for part in range(PARTS):
        lax.fori_loop(max(part * PEERS, 1), (part + 1) * PEERS, send, part)
    arrived[0] = outgoing[0]

    get_sg.wait()
    get_su.wait()
    get_sd.wait()
    hidden = dot(normed[...], sg[...])
    hidden = hidden / (1.0 + jnp.exp(-hidden)) * dot(normed[...], su[...])
    hidden = hidden.astype(BF16)
    for n in range(0, D, 512):
        acc[:, n : n + 512] = settled[:, n : n + 512].astype(F32) + dot(hidden, sd[:, n : n + 512])

    get_eg.wait()
    get_eu.wait()
    get_ed.wait()

    def span(refs, sems_send, sem_recv, first, count):
        src, dst = refs
        return pltpu.make_async_remote_copy(
            src.at[pl.ds(first, count), pl.ds(0, CAP)], dst.at[pl.ds(first, count), pl.ds(0, CAP)],
            sems_send, sem_recv, device_id=(sp, 1 - tp), device_id_type=MESH,
        )

    for part in range(PARTS):
        first = max(part * PEERS, 1)
        count = (part + 1) * PEERS - first
        span((outgoing, arrived), out_send, out_recv.at[part], first, count).wait_recv()
        base = part * PEERS
        rows = arrived[pl.ds(base, PEERS)].reshape(PEERS * SLOTS, D)
        hidden = dot(rows, eg[...])
        hidden = hidden / (1.0 + jnp.exp(-hidden)) * dot(rows, eu[...])
        hidden = hidden.astype(BF16)
        for n in range(0, D, 512):
            value = dot(hidden, ed[:, n : n + 512]).astype(BF16)
            results[pl.ds(base, PEERS), :, n : n + 512] = value.reshape(PEERS, SLOTS, 512)
        lax.fori_loop(first, base + PEERS, send_back, part)
    returned[0] = results[0]

    for part in range(PARTS):
        first = max(part * PEERS, 1)
        count = (part + 1) * PEERS - first
        span((results, returned), back_send, back_recv.at[part], first, count).wait_recv()
        base = part * PEERS
        factors = comb[pl.ds(base * SLOTS, PEERS * SLOTS), :].T
        for n in range(0, D, 512):
            rows = returned[pl.ds(base, PEERS), :, n : n + 512].reshape(PEERS * SLOTS, 512)
            both = dot(factors, rows)
            value = acc[:, n : n + 512] + (both[:TOKENS_HERE] + both[TOKENS_HERE:])
            if part < PARTS - 1:
                acc[:, n : n + 512] = value
            else:
                out_ref[:, n : n + 512] = value.astype(BF16)

    span((outgoing, arrived), out_send, out_recv.at[0], 1, DEVICES - 1).wait_send()
    span((results, returned), back_send, back_recv.at[0], 1, DEVICES - 1).wait_send()


def on_device(
    residual, pool_input, group_maps, pool_scale, out_proj, norm_gain,
    shared_gate, shared_up, shared_down, expert_gate, expert_up, expert_down,
    expert_ids, route_score,
):
    any_space = pl.BlockSpec(memory_space=pl.ANY)
    vmem = pltpu.VMEM
    block = (DEVICES, SLOTS, D)
    return pl.pallas_call(
        kernel,
        name="mixer_experts",
        out_shape=jax.ShapeDtypeStruct((TOKENS_HERE, D), BF16),
        in_specs=[any_space] * 14,
        out_specs=pl.BlockSpec(memory_space=pltpu.VMEM),
        scratch_shapes=[
            vmem((TOKENS_HERE, D), BF16),
            vmem((REACH + ROWS, CHANNELS), BF16),
            vmem((GROUPS, GW, GW), BF16),
            vmem((8, 128), F32),
            vmem((2 * CHANNELS, D), BF16),
            vmem((D // 128, 128), F32),
            vmem((D, HID), BF16),
            vmem((D, HID), BF16),
            vmem((HID, D), BF16),
            vmem((D, HID), BF16),
            vmem((D, HID), BF16),
            vmem((HID, D), BF16),
            vmem((TOPK, TOKENS_HERE), jnp.int32),
            vmem((TOPK, TOKENS_HERE), F32),
            vmem((ROWS, CHANNELS), BF16),
            vmem((TOKENS_HERE, CHANNELS), BF16),
            vmem((TOKENS_HERE, D), BF16),
            vmem((TOKENS_HERE, D), BF16),
            vmem((TOKENS_HERE, D), F32),
            vmem((DEVICES * SLOTS, TOKENS_HERE), BF16),
            vmem((DEVICES * SLOTS, 2 * TOKENS_HERE), BF16),
            vmem(block, BF16),
            vmem(block, BF16),
            vmem(block, BF16),
            vmem(block, BF16),
            pltpu.SemaphoreType.DMA((14,)),
            pltpu.SemaphoreType.DMA,
            pltpu.SemaphoreType.DMA,
            pltpu.SemaphoreType.DMA,
            pltpu.SemaphoreType.DMA,
            pltpu.SemaphoreType.DMA,
            pltpu.SemaphoreType.DMA((PARTS,)),
            pltpu.SemaphoreType.DMA,
            pltpu.SemaphoreType.DMA((PARTS,)),
        ],
        compiler_params=pltpu.CompilerParams(
            collective_id=0, has_side_effects=True, vmem_limit_bytes=60 << 20
        ),
    )(
        residual, pool_input, group_maps, pool_scale.reshape(8, 128), out_proj,
        norm_gain.reshape(D // 128, 128), shared_gate, shared_up, shared_down,
        expert_gate, expert_up, expert_down, expert_ids.T, route_score.T,
    )


def solution(mesh):
    in_specs = (
        P(("sp", "tp"), None),
        P("sp", "tp"),
        P(), P(), P(), P(), P(), P(), P(),
        P(("sp", "tp"), None, None),
        P(("sp", "tp"), None, None),
        P(("sp", "tp"), None, None),
        P(("sp", "tp"), None),
        P(("sp", "tp"), None),
    )
    return jax.shard_map(
        on_device, mesh=mesh, in_specs=in_specs, out_specs=P(("sp", "tp"), None), check_vma=False
    )
```

time: 197 us -> 98.3 us (0.50)
  Pallas kernels: 0 us -> 95.7 us
  blocking collectives: 67.3 us -> 0 us
  waiting for transfers between devices: 50.5 us -> 0 us
  local copies, waits for them, and re-layouts: 42.2 us -> 1.88 us
  matrix products: 25.3 us -> 0 us
  starting transfers between devices: 9.56 us -> 0 us
    pallas_call x0 -> x1, Pallas kernels: none -> 95.7 us  [on_device(): pl.pallas_call(kernel, name='mixer_experts', out_shape=jax.ShapeDtypeStru...]
    all_to_all x2 -> x0, blocking collectives: 67.3 us -> none  [the longest x1 62.8 us: on_device(): lax.all_to_all(outgoing, ('sp', 'tp'), split_axis=1, concat_axis=1, tiled...]
    all_to_all x1 -> x0, waiting for transfers between devices: 50.5 us -> none  [on_device(): lax.all_to_all(results, ('sp', 'tp'), split_axis=1, concat_axis=1, tiled=...]
    dot_general x8 -> x0, matrix products: 25.3 us -> none  [the longest x2 12.8 us: swiglu(): return jnp.dot(hidden, w_down, preferred_element_type=jnp.float32)]
    reshape x5 -> x0, local copies, waits for them, and re-layouts: 13.7 us -> none  [the longest x1 5.63 us: on_device(): results = expert_rows.reshape(item_total, experts, model_width)]
    gather x2 -> x0, local copies, waits for them, and re-layouts: 11.8 us -> none  [the longest x1 7.58 us: on_device(): returned.reshape(capacity * experts, model_width)[slot_index]]
    all_to_all x2 -> x0, local copies, waits for them, and re-layouts: 7.31 us -> none  [the longest x1 5.59 us: on_device(): lax.all_to_all(results, ('sp', 'tp'), split_axis=1, concat_axis=1, tiled=...]
    all_to_all x1 -> x0, starting transfers between devices: 5.64 us -> none  [on_device(): lax.all_to_all(results, ('sp', 'tp'), split_axis=1, concat_axis=1, tiled=...]
  transfers between devices with their start and end apart: 2 -> 0, of which waited for: 1 -> 0; matrix products, arithmetic and copies ran while one was open for 4% -> 0% of each run, Pallas kernels for 0% -> 0%
where the time goes in v1:
time: 98.3 us; the launch traced here: 97.6 us
  Pallas kernels  95.7 us (97%)
  local copies, waits for them, and re-layouts  1.88 us (2%)
    pallas_call x1, Pallas kernels, on_device(): pl.pallas_call(kernel, name='mixer_experts', out_shape=jax.ShapeDtypeStru...  95.7 us

profile of v1, /device:TPU:1, one launch (start us, length us, event | category | flops | bytes accessed | tf_op | source)
XLA Modules:
  0.0 97.6 jit_solution(15098772996672107519)
XLA Ops:
  0.0 95.7 %mixer_experts.1 = bf16[128,2048]{1,0:T(8,128)(2,1)} custom-call(bf16[128,2048]{1,0:T(8,128)(2,1)} %res_hbm.1, bf16[256,512]{1,0:T(8,128)(2,1)} %pool_hbm.1, bf16[8,128,128]{2,1,0:T(8,128)(2,1)} %maps_hbm.1, f32[8,128]{1,0:T(8,128)} %bitcast.5, bf16[1024,2048]{1,0:T(8,128)(2,1)} %proj_hbm.1, f32[16,128]{1,0:T(8,128)} %bitcast.4, bf16[2048,512]{1,0:T(8,128)(2,1)} %sg_hbm.1, ...), custom_call_target="tpu_custom_call" | custom-call | tf_op jit(solution)/shard_map/mixer_experts/pallas_call | solution.py:278
  95.7 1.9 %copy.16 = bf16[128,2048]{1,0:T(8,128)(2,1)} copy(bf16[128,2048]{1,0:T(8,128)(2,1)} %mixer_experts.1) | data formatting | bytes 1048576

commit v2 on v1

--- a/solution.py
+++ b/solution.py
@@ -29,8 +29,12 @@
 GW = 128
 REACH = 16
 STRIDE = 53
-PARTS = 4
-PEERS = DEVICES // PARTS
+PARTS = (32, 32, 32, 16, 16)
+
+
+def members(part):
+    first = sum(PARTS[:part])
+    return range(max(first, 1), first + PARTS[part])
 
 
 def dot(a, b):
@@ -38,24 +42,26 @@
 
 
 def offset_of(k):
-    kk = lax.rem(k * STRIDE, DEVICES)
-    c = lax.rem(kk, 2)
-    x = lax.rem(lax.div(kk, 2), SIDE)
-    y = lax.rem(lax.div(kk, 8), SIDE)
-    z = lax.div(kk, 32)
-    return z, y, x, c
-
-
-def shifted(sp, tp, k, sign):
-    dz, dy, dx, dc = offset_of(k)
-    z = lax.div(sp, SIDE * SIDE)
-    y = lax.rem(lax.div(sp, SIDE), SIDE)
-    x = lax.rem(sp, SIDE)
-    z = lax.rem(z + sign * dz + SIDE, SIDE)
-    y = lax.rem(y + sign * dy + SIDE, SIDE)
-    x = lax.rem(x + sign * dx + SIDE, SIDE)
-    c = lax.rem(tp + dc, 2)
-    return (z * SIDE + y) * SIDE + x, c
+    kk = k * STRIDE % DEVICES
+    return kk // 32, kk // 8 % SIDE, kk // 2 % SIDE, kk % 2
+
+
+class Place:
+    def __init__(self):
+        self.sp = lax.axis_index("sp")
+        self.tp = lax.axis_index("tp")
+        z, y, x = self.sp // 16, self.sp // SIDE % SIDE, self.sp % SIDE
+        self.z = [(z + d) % SIDE * 16 for d in range(SIDE)]
+        self.y = [(y + d) % SIDE * SIDE for d in range(SIDE)]
+        self.x = [(x + d) % SIDE for d in range(SIDE)]
+        self.c = [self.tp, 1 - self.tp]
+
+    def at(self, dz, dy, dx, dc):
+        return self.z[dz % SIDE] + self.y[dy % SIDE] + self.x[dx % SIDE], self.c[dc]
+
+    def peer(self, k, sign):
+        dz, dy, dx, dc = offset_of(k)
+        return self.at(sign * dz, sign * dy, sign * dx, dc)
 
 
 def kernel(
@@ -66,10 +72,10 @@
     mix, halves, settled, normed, acc, place, comb,
     outgoing, arrived, results, returned,
     in_sems, halo_send, halo_recv, swap_send, swap_recv,
-    out_send, out_recv, back_send, back_recv,
+    out_send, out_recv, back_send, back_recv, plane_sem, cube_sem,
 ):
-    sp = lax.axis_index("sp")
-    tp = lax.axis_index("tp")
+    here = Place()
+    sp, tp = here.sp, here.tp
 
     def fetch(i, src, dst):
         copy = pltpu.make_async_copy(src, dst, in_sems.at[i])
@@ -91,27 +97,30 @@
     get_eu = fetch(12, eu_hbm.at[0], eu)
     get_ed = fetch(13, ed_hbm.at[0], ed)
 
+    barrier = pltpu.get_barrier_semaphore()
+    near = [here.at(0, 0, d // 2, d % 2) for d in range(1, 2 * SIDE)]
+    near += [here.at(0, d, 0, 0) for d in range(1, SIDE)]
+    near += [here.at(d, 0, 0, 0) for d in range(1, SIDE)]
+    following = (sp + 1) % (DEVICES // 2)
+    near += [(following, tp), ((sp + DEVICES // 2 - 1) % (DEVICES // 2), tp)]
+    for device in near:
+        pl.semaphore_signal(barrier, inc=1, device_id=device, device_id_type=MESH)
+
     def clear(i, _):
-        returned[pl.ds(i * 8, 8)] = jnp.zeros((8, SLOTS, D), BF16)
+        returned[pl.ds(i * 8, 8), CAP:, :] = jnp.zeros((8, SLOTS - CAP, D), BF16)
         return 0
 
     lax.fori_loop(0, DEVICES // 8, clear, 0)
-
-    barrier = pltpu.get_barrier_semaphore()
-
-    def greet(k, _):
-        pl.semaphore_signal(barrier, inc=1, device_id=shifted(sp, tp, k, 1), device_id_type=MESH)
-        return 0
-
-    lax.fori_loop(1, DEVICES, greet, 0)
     get_pool.wait()
-    pl.semaphore_wait(barrier, DEVICES - 1)
+    pl.semaphore_wait(barrier, len(near))
 
     halo = pltpu.make_async_remote_copy(
         ext.at[pl.ds(ROWS, REACH)], ext.at[pl.ds(0, REACH)], halo_send, halo_recv,
-        device_id=(lax.rem(sp + 1, DEVICES // 2), tp), device_id_type=MESH,
+        device_id=(following, tp), device_id_type=MESH,
     )
     halo.start()
+    for d in range(1, SIDE):
+        pl.semaphore_signal(plane_sem, inc=1, device_id=here.at(0, d, 0, 0), device_id_type=MESH)
 
     get_ids.wait()
     get_score.wait()
@@ -131,14 +140,22 @@
     tag = chosen * (rank + 1.0)
     slot_row = lax.broadcasted_iota(jnp.int32, (DEVICES * SLOTS, DEVICES), 0)
     slot_expert = lax.broadcasted_iota(jnp.int32, (DEVICES * SLOTS, DEVICES), 1)
-    peer_sp, peer_tp = shifted(sp, tp, lax.div(slot_row, SLOTS), 1)
-    spread = (peer_sp * 2 + peer_tp == slot_expert).astype(BF16)
-    slot_number = (lax.rem(slot_row, SLOTS) + 1).astype(F32)
+    turn = (slot_row // SLOTS) * STRIDE % DEVICES
+    peer_z = (sp // 16 + turn // 32) % SIDE
+    peer_y = (sp // SIDE + turn // 8) % SIDE
+    peer_x = (sp + turn // 2) % SIDE
+    peer = ((peer_z * SIDE + peer_y) * SIDE + peer_x) * 2 + (tp + turn) % 2
+    spread = (peer == slot_expert).astype(BF16)
+    slot_number = (slot_row % SLOTS + 1).astype(F32)
     place[...] = (dot(spread, tag.astype(BF16)) == slot_number).astype(BF16)
     weight_high = weight.astype(BF16)
     weight_low = (weight - weight_high.astype(F32)).astype(BF16)
     comb[:, :TOKENS_HERE] = dot(spread, weight_high).astype(BF16) * place[...]
     comb[:, TOKENS_HERE:] = dot(spread, weight_low).astype(BF16) * place[...]
+
+    pl.semaphore_wait(plane_sem, SIDE - 1)
+    for d in range(1, SIDE):
+        pl.semaphore_signal(cube_sem, inc=1, device_id=here.at(d, 0, 0, 0), device_id_type=MESH)
 
     get_maps.wait()
     get_scale.wait()
@@ -193,24 +210,14 @@
 
     lax.fori_loop(0, D // 256, fill, 0)
 
-    def send(k, part):
-        pltpu.make_async_remote_copy(
-            outgoing.at[k, pl.ds(0, CAP)], arrived.at[k, pl.ds(0, CAP)],
-            out_send, out_recv.at[part],
-            device_id=shifted(sp, tp, k, 1), device_id_type=MESH,
-        ).start()
-        return part
-
-    def send_back(k, part):
-        pltpu.make_async_remote_copy(
-            results.at[k, pl.ds(0, CAP)], returned.at[k, pl.ds(0, CAP)],
-            back_send, back_recv.at[part],
-            device_id=shifted(sp, tp, k, -1), device_id_type=MESH,
-        ).start()
-        return part
-
-    for part in range(PARTS):
-        lax.fori_loop(max(part * PEERS, 1), (part + 1) * PEERS, send, part)
+    pl.semaphore_wait(cube_sem, SIDE - 1)
+    for part in range(len(PARTS)):
+        for k in members(part):
+            pltpu.make_async_remote_copy(
+                outgoing.at[k, pl.ds(0, CAP)], arrived.at[k, pl.ds(0, CAP)],
+                out_send, out_recv.at[part],
+                device_id=here.peer(k, 1), device_id_type=MESH,
+            ).start()
     arrived[0] = outgoing[0]
 
     get_sg.wait()
@@ -226,45 +233,49 @@
     get_eu.wait()
     get_ed.wait()
 
-    def span(refs, sems_send, sem_recv, first, count):
-        src, dst = refs
+    def span(src, dst, send_sem, recv_sem, first, count):
         return pltpu.make_async_remote_copy(
             src.at[pl.ds(first, count), pl.ds(0, CAP)], dst.at[pl.ds(first, count), pl.ds(0, CAP)],
-            sems_send, sem_recv, device_id=(sp, 1 - tp), device_id_type=MESH,
+            send_sem, recv_sem, device_id=(sp, 1 - tp), device_id_type=MESH,
         )
 
-    for part in range(PARTS):
-        first = max(part * PEERS, 1)
-        count = (part + 1) * PEERS - first
-        span((outgoing, arrived), out_send, out_recv.at[part], first, count).wait_recv()
-        base = part * PEERS
-        rows = arrived[pl.ds(base, PEERS)].reshape(PEERS * SLOTS, D)
+    base = 0
+    for part, size in enumerate(PARTS):
+        ks = members(part)
+        span(outgoing, arrived, out_send, out_recv.at[part], ks[0], len(ks)).wait_recv()
+        rows = arrived[pl.ds(base, size)].reshape(size * SLOTS, D)
         hidden = dot(rows, eg[...])
         hidden = hidden / (1.0 + jnp.exp(-hidden)) * dot(rows, eu[...])
         hidden = hidden.astype(BF16)
         for n in range(0, D, 512):
             value = dot(hidden, ed[:, n : n + 512]).astype(BF16)
-            results[pl.ds(base, PEERS), :, n : n + 512] = value.reshape(PEERS, SLOTS, 512)
-        lax.fori_loop(first, base + PEERS, send_back, part)
+            results[pl.ds(base, size), :, n : n + 512] = value.reshape(size, SLOTS, 512)
+        for k in ks:
+            pltpu.make_async_remote_copy(
+                results.at[k, pl.ds(0, CAP)], returned.at[k, pl.ds(0, CAP)],
+                back_send, back_recv.at[part],
+                device_id=here.peer(k, -1), device_id_type=MESH,
+            ).start()
+        base += size
     returned[0] = results[0]
 
-    for part in range(PARTS):
-        first = max(part * PEERS, 1)
-        count = (part + 1) * PEERS - first
-        span((results, returned), back_send, back_recv.at[part], first, count).wait_recv()
-        base = part * PEERS
-        factors = comb[pl.ds(base * SLOTS, PEERS * SLOTS), :].T
+    base = 0
+    for part, size in enumerate(PARTS):
+        ks = members(part)
+        span(results, returned, back_send, back_recv.at[part], ks[0], len(ks)).wait_recv()
+        factors = comb[pl.ds(base * SLOTS, size * SLOTS), :].T
         for n in range(0, D, 512):
-            rows = returned[pl.ds(base, PEERS), :, n : n + 512].reshape(PEERS * SLOTS, 512)
+            rows = returned[pl.ds(base, size), :, n : n + 512].reshape(size * SLOTS, 512)
             both = dot(factors, rows)
             value = acc[:, n : n + 512] + (both[:TOKENS_HERE] + both[TOKENS_HERE:])
-            if part < PARTS - 1:
+            if part < len(PARTS) - 1:
                 acc[:, n : n + 512] = value
             else:
                 out_ref[:, n : n + 512] = value.astype(BF16)
-
-    span((outgoing, arrived), out_send, out_recv.at[0], 1, DEVICES - 1).wait_send()
-    span((results, returned), back_send, back_recv.at[0], 1, DEVICES - 1).wait_send()
+        base += size
+
+    span(outgoing, arrived, out_send, out_recv.at[0], 1, DEVICES - 1).wait_send()
+    span(results, returned, back_send, back_recv.at[0], 1, DEVICES - 1).wait_send()
 
 
 def on_device(
@@ -313,9 +324,11 @@
             pltpu.SemaphoreType.DMA,
             pltpu.SemaphoreType.DMA,
             pltpu.SemaphoreType.DMA,
-            pltpu.SemaphoreType.DMA((PARTS,)),
-            pltpu.SemaphoreType.DMA,
-            pltpu.SemaphoreType.DMA((PARTS,)),
+            pltpu.SemaphoreType.DMA((len(PARTS),)),
+            pltpu.SemaphoreType.DMA,
+            pltpu.SemaphoreType.DMA((len(PARTS),)),
+            pltpu.SemaphoreType.REGULAR,
+            pltpu.SemaphoreType.REGULAR,
         ],
         compiler_params=pltpu.CompilerParams(
             collective_id=0, has_side_effects=True, vmem_limit_bytes=60 << 20

time: 98.3 us -> 94 us (0.956)
  Pallas kernels: 95.7 us -> 91.5 us
    pallas_call x1, Pallas kernels: 95.7 us -> 91.5 us  [on_device(): pl.pallas_call(kernel, name='mixer_experts', out_shape=jax.ShapeDtypeStru...]
where the time goes in v2:
time: 94 us; the launch traced here: 93.4 us
  Pallas kernels  91.5 us (97%)
  local copies, waits for them, and re-layouts  1.88 us (2%)
    pallas_call x1, Pallas kernels, on_device(): pl.pallas_call(kernel, name='mixer_experts', out_shape=jax.ShapeDtypeStru...  91.5 us
    unnamed x1, local copies, waits for them, and re-layouts  1.88 us

profile of v2, /device:TPU:1, one launch (start us, length us, event | category | flops | bytes accessed | tf_op | source)
XLA Modules:
  0.0 93.4 jit_solution(16490062976432829581)
XLA Ops:
  0.0 91.5 %mixer_experts.1 = bf16[128,2048]{1,0:T(8,128)(2,1)} custom-call(bf16[128,2048]{1,0:T(8,128)(2,1)} %res_hbm.1, bf16[256,512]{1,0:T(8,128)(2,1)} %pool_hbm.1, bf16[8,128,128]{2,1,0:T(8,128)(2,1)} %maps_hbm.1, f32[8,128]{1,0:T(8,128)} %bitcast.5, bf16[1024,2048]{1,0:T(8,128)(2,1)} %proj_hbm.1, f32[16,128]{1,0:T(8,128)} %bitcast.4, bf16[2048,512]{1,0:T(8,128)(2,1)} %sg_hbm.1, ...), custom_call_target="tpu_custom_call" | custom-call | tf_op jit(solution)/shard_map/mixer_experts/pallas_call | solution.py:289
  91.5 1.9 %copy.16 = bf16[128,2048]{1,0:T(8,128)(2,1)} copy(bf16[128,2048]{1,0:T(8,128)(2,1)} %mixer_experts.1) | data formatting | bytes 1048576

commit v3 on v2

--- a/solution.py
+++ b/solution.py
@@ -29,7 +29,7 @@
 GW = 128
 REACH = 16
 STRIDE = 53
-PARTS = (32, 32, 32, 16, 16)
+PARTS = (16, 16, 32, 32, 16, 16)
 
 
 def members(part):
@@ -69,7 +69,7 @@
     sg_hbm, su_hbm, sd_hbm, eg_hbm, eu_hbm, ed_hbm, ids_hbm, score_hbm,
     out_ref,
     res, ext, maps, scale, proj, gain, sg, su, sd, eg, eu, ed, ids, score,
-    mix, halves, settled, normed, acc, place, comb,
+    mix, other_ext, halo, settled, normed, acc, place, comb,
     outgoing, arrived, results, returned,
     in_sems, halo_send, halo_recv, swap_send, swap_recv,
     out_send, out_recv, back_send, back_recv, plane_sem, cube_sem,
@@ -77,6 +77,16 @@
     here = Place()
     sp, tp = here.sp, here.tp
 
+    barrier = pltpu.get_barrier_semaphore()
+    near = [here.at(0, 0, d // 2, d % 2) for d in range(1, 2 * SIDE)]
+    near += [here.at(0, d, 0, 0) for d in range(1, SIDE)]
+    near += [here.at(d, 0, 0, 0) for d in range(1, SIDE)]
+    following = (sp + 1) % (DEVICES // 2)
+    previous = (sp + DEVICES // 2 - 1) % (DEVICES // 2)
+    near += [(following, 0), (following, 1), (previous, 0), (previous, 1)]
+    for device in near:
+        pl.semaphore_signal(barrier, inc=1, device_id=device, device_id_type=MESH)
+
     def fetch(i, src, dst):
         copy = pltpu.make_async_copy(src, dst, in_sems.at[i])
         copy.start()
@@ -85,42 +95,40 @@
     get_pool = fetch(0, pool_hbm, ext.at[pl.ds(REACH, ROWS)])
     get_ids = fetch(1, ids_hbm, ids)
     get_score = fetch(2, score_hbm, score)
-    get_maps = fetch(3, maps_hbm.at[pl.ds(tp * GROUPS, GROUPS)], maps)
+    get_maps = fetch(3, maps_hbm, maps)
     get_scale = fetch(4, scale_hbm, scale)
     get_res = fetch(5, res_hbm, res)
     get_gain = fetch(6, gain_hbm, gain)
     get_proj = fetch(7, proj_hbm, proj)
+    ext[:REACH, :] = jnp.zeros((REACH, CHANNELS), BF16)
+    pl.semaphore_wait(barrier, len(near))
+    for d in range(1, SIDE):
+        pl.semaphore_signal(plane_sem, inc=1, device_id=here.at(0, d, 0, 0), device_id_type=MESH)
+    get_pool.wait()
+
+    def slab(core):
+        return pl.ds(pl.multiple_of(core * TOKENS_HERE, TOKENS_HERE), REACH + TOKENS_HERE)
+
+    swap = pltpu.make_async_remote_copy(
+        ext.at[slab(1 - tp)], other_ext, swap_send, swap_recv,
+        device_id=(sp, 1 - tp), device_id_type=MESH,
+    )
+    halos = [
+        pltpu.make_async_remote_copy(
+            ext.at[pl.ds(ROWS, REACH)], halo.at[i], halo_send.at[i], halo_recv.at[i],
+            device_id=(following, [tp, 1 - tp][i]), device_id_type=MESH,
+        )
+        for i in range(2)
+    ]
+    halos[0].start()
+    halos[1].start()
+    swap.start()
     get_sg = fetch(8, sg_hbm, sg)
     get_su = fetch(9, su_hbm, su)
     get_sd = fetch(10, sd_hbm, sd)
     get_eg = fetch(11, eg_hbm.at[0], eg)
     get_eu = fetch(12, eu_hbm.at[0], eu)
     get_ed = fetch(13, ed_hbm.at[0], ed)
-
-    barrier = pltpu.get_barrier_semaphore()
-    near = [here.at(0, 0, d // 2, d % 2) for d in range(1, 2 * SIDE)]
-    near += [here.at(0, d, 0, 0) for d in range(1, SIDE)]
-    near += [here.at(d, 0, 0, 0) for d in range(1, SIDE)]
-    following = (sp + 1) % (DEVICES // 2)
-    near += [(following, tp), ((sp + DEVICES // 2 - 1) % (DEVICES // 2), tp)]
-    for device in near:
-        pl.semaphore_signal(barrier, inc=1, device_id=device, device_id_type=MESH)
-
-    def clear(i, _):
-        returned[pl.ds(i * 8, 8), CAP:, :] = jnp.zeros((8, SLOTS - CAP, D), BF16)
-        return 0
-
-    lax.fori_loop(0, DEVICES // 8, clear, 0)
-    get_pool.wait()
-    pl.semaphore_wait(barrier, len(near))
-
-    halo = pltpu.make_async_remote_copy(
-        ext.at[pl.ds(ROWS, REACH)], ext.at[pl.ds(0, REACH)], halo_send, halo_recv,
-        device_id=(following, tp), device_id_type=MESH,
-    )
-    halo.start()
-    for d in range(1, SIDE):
-        pl.semaphore_signal(plane_sem, inc=1, device_id=here.at(0, d, 0, 0), device_id_type=MESH)
 
     get_ids.wait()
     get_score.wait()
@@ -159,40 +167,46 @@
 
     get_maps.wait()
     get_scale.wait()
-    halo.wait()
-    center = lax.broadcasted_iota(jnp.int32, (ROWS, REACH + ROWS), 0) + REACH
-    other = lax.broadcasted_iota(jnp.int32, (ROWS, REACH + ROWS), 1)
-    real = (other >= REACH) | (sp > 0)
-    position = sp * ROWS + lax.broadcasted_iota(jnp.int32, (ROWS, GW), 0)
-    for g in range(GROUPS):
-        lanes = slice(g * GW, (g + 1) * GW)
-        band = (other <= center) & (other > center - windows[g]) & real
-        total = dot(band.astype(BF16), ext[:, lanes])
-        divisor = jnp.minimum(position + 1, windows[g]).astype(F32)
-        contrast = (total / divisor - ext[REACH:, lanes].astype(F32)).astype(BF16)
-        mapped = dot(contrast, maps[g])
-        row_scale = jnp.where(tp == 0, scale[g : g + 1, :], scale[GROUPS + g : GROUPS + g + 1, :])
-        mix[:, lanes] = (mapped * row_scale).astype(BF16)
-
-    swap = pltpu.make_async_remote_copy(
-        mix.at[pl.ds(pl.multiple_of((1 - tp) * TOKENS_HERE, TOKENS_HERE), TOKENS_HERE)],
-        halves, swap_send, swap_recv, device_id=(sp, 1 - tp), device_id_type=MESH,
-    )
-    swap.start()
-
+    first = sp * ROWS + tp * TOKENS_HERE
+    center = lax.broadcasted_iota(jnp.int32, (TOKENS_HERE, REACH + TOKENS_HERE), 0) + REACH
+    source = lax.broadcasted_iota(jnp.int32, (TOKENS_HERE, REACH + TOKENS_HERE), 1)
+    real = (source >= REACH) | (first > 0)
+    position = first + lax.broadcasted_iota(jnp.int32, (TOKENS_HERE, GW), 0)
+
+    def mix_half(i):
+        core = [tp, 1 - tp][i]
+        rows = ext[slab(tp), :] if i == 0 else other_ext[...]
+        head = jnp.where(tp == 0, halo[i].astype(F32), rows[:REACH].astype(F32)).astype(BF16)
+        rows = jnp.concatenate([head, rows[REACH:]], axis=0)
+        for g in range(GROUPS):
+            lanes = slice(g * GW, (g + 1) * GW)
+            band = (source <= center) & (source > center - windows[g]) & real
+            total = dot(band.astype(BF16), rows[:, lanes])
+            divisor = jnp.minimum(position + 1, windows[g]).astype(F32)
+            contrast = (total / divisor - rows[REACH:, lanes].astype(F32)).astype(BF16)
+            mapped = dot(contrast, maps[core * GROUPS + g])
+            low, high = scale[g : g + 1, :], scale[GROUPS + g : GROUPS + g + 1, :]
+            mix[:, lanes] = (mapped * jnp.where(core == 0, low, high)).astype(BF16)
+
+    def proj_half(i, n):
+        core = [tp, 1 - tp][i]
+        part = pl.ds(pl.multiple_of(core * CHANNELS, CHANNELS), CHANNELS)
+        return dot(mix[...], proj[part, n : n + 512])
+
+    halos[0].wait()
+    mix_half(0)
     get_res.wait()
     get_gain.wait()
     get_proj.wait()
-    own = mix[pl.ds(pl.multiple_of(tp * TOKENS_HERE, TOKENS_HERE), TOKENS_HERE), :]
     for n in range(0, D, 512):
-        near = proj[pl.ds(pl.multiple_of(tp * CHANNELS, CHANNELS), CHANNELS), n : n + 512]
-        acc[:, n : n + 512] = dot(own, near)
+        acc[:, n : n + 512] = res[:, n : n + 512].astype(F32) + proj_half(0, n)
+    halos[1].wait()
     swap.wait()
+    mix_half(1)
+
     square = jnp.zeros((TOKENS_HERE, 1), F32)
     for n in range(0, D, 512):
-        far = proj[pl.ds(pl.multiple_of((1 - tp) * CHANNELS, CHANNELS), CHANNELS), n : n + 512]
-        value = acc[:, n : n + 512] + dot(halves[...], far)
-        value = (value + res[:, n : n + 512].astype(F32)).astype(BF16)
+        value = (acc[:, n : n + 512] + proj_half(1, n)).astype(BF16)
         settled[:, n : n + 512] = value
         value = value.astype(F32)
         square = square + jnp.sum(value * value, axis=1, keepdims=True)
@@ -202,16 +216,14 @@
         value = settled[:, lanes].astype(F32) * inverse * gain[j : j + 1, :]
         normed[:, lanes] = value.astype(BF16)
 
-    def fill(i, _):
-        n = pl.multiple_of(i * 256, 256)
-        rows = dot(place[...], normed[:, pl.ds(n, 256)]).astype(BF16)
-        outgoing[:, :, pl.ds(n, 256)] = rows.reshape(DEVICES, SLOTS, 256)
-        return 0
-
-    lax.fori_loop(0, D // 256, fill, 0)
-
-    pl.semaphore_wait(cube_sem, SIDE - 1)
-    for part in range(len(PARTS)):
+    base = 0
+    for part, size in enumerate(PARTS):
+        for n in range(0, D, 512):
+            rows = dot(place[pl.ds(base * SLOTS, size * SLOTS), :], normed[:, n : n + 512])
+            outgoing[pl.ds(base, size), :, n : n + 512] = rows.astype(BF16).reshape(size, SLOTS, 512)
+        base += size
+        if part == 0:
+            pl.semaphore_wait(cube_sem, SIDE - 1)
         for k in members(part):
             pltpu.make_async_remote_copy(
                 outgoing.at[k, pl.ds(0, CAP)], arrived.at[k, pl.ds(0, CAP)],
@@ -219,6 +231,12 @@
                 device_id=here.peer(k, 1), device_id_type=MESH,
             ).start()
     arrived[0] = outgoing[0]
+
+    def clear(i, _):
+        returned[pl.ds(i * 8, 8), CAP:, :] = jnp.zeros((8, SLOTS - CAP, D), BF16)
+        return 0
+
+    lax.fori_loop(0, DEVICES // 8, clear, 0)
 
     get_sg.wait()
     get_su.wait()
@@ -295,7 +313,7 @@
         scratch_shapes=[
             vmem((TOKENS_HERE, D), BF16),
             vmem((REACH + ROWS, CHANNELS), BF16),
-            vmem((GROUPS, GW, GW), BF16),
+            vmem((2 * GROUPS, GW, GW), BF16),
             vmem((8, 128), F32),
             vmem((2 * CHANNELS, D), BF16),
             vmem((D // 128, 128), F32),
@@ -307,8 +325,9 @@
             vmem((HID, D), BF16),
             vmem((TOPK, TOKENS_HERE), jnp.int32),
             vmem((TOPK, TOKENS_HERE), F32),
-            vmem((ROWS, CHANNELS), BF16),
             vmem((TOKENS_HERE, CHANNELS), BF16),
+            vmem((REACH + TOKENS_HERE, CHANNELS), BF16),
+            vmem((2, REACH, CHANNELS), BF16),
             vmem((TOKENS_HERE, D), BF16),
             vmem((TOKENS_HERE, D), BF16),
             vmem((TOKENS_HERE, D), F32),
@@ -319,8 +338,8 @@
             vmem(block, BF16),
             vmem(block, BF16),
             pltpu.SemaphoreType.DMA((14,)),
-            pltpu.SemaphoreType.DMA,
-            pltpu.SemaphoreType.DMA,
+            pltpu.SemaphoreType.DMA((2,)),
+            pltpu.SemaphoreType.DMA((2,)),
             pltpu.SemaphoreType.DMA,
             pltpu.SemaphoreType.DMA,
             pltpu.SemaphoreType.DMA,

time: 94 us -> 88 us (0.936)
  Pallas kernels: 91.5 us -> 86 us
    pallas_call x1, Pallas kernels: 91.5 us -> 86 us  [on_device(): pl.pallas_call(kernel, name='mixer_experts', out_shape=jax.ShapeDtypeStru...]
where the time goes in v3:
time: 88 us; the launch traced here: 87.9 us
  Pallas kernels  86 us (98%)
  local copies, waits for them, and re-layouts  1.88 us (2%)
    pallas_call x1, Pallas kernels, on_device(): pl.pallas_call(kernel, name='mixer_experts', out_shape=jax.ShapeDtypeStru...  86 us
    unnamed x1, local copies, waits for them, and re-layouts  1.88 us

profile of v3, /device:TPU:1, one launch (start us, length us, event | category | flops | bytes accessed | tf_op | source)
XLA Modules:
  0.0 87.9 jit_solution(4365826340028030215)
XLA Ops:
  0.0 86.0 %mixer_experts.1 = bf16[128,2048]{1,0:T(8,128)(2,1)} custom-call(bf16[128,2048]{1,0:T(8,128)(2,1)} %res_hbm.1, bf16[256,512]{1,0:T(8,128)(2,1)} %pool_hbm.1, bf16[8,128,128]{2,1,0:T(8,128)(2,1)} %maps_hbm.1, f32[8,128]{1,0:T(8,128)} %bitcast.5, bf16[1024,2048]{1,0:T(8,128)(2,1)} %proj_hbm.1, f32[16,128]{1,0:T(8,128)} %bitcast.4, bf16[2048,512]{1,0:T(8,128)(2,1)} %sg_hbm.1, ...), custom_call_target="tpu_custom_call" | custom-call | tf_op jit(solution)/shard_map/mixer_experts/pallas_call | solution.py:307
  86.0 1.9 %copy.16 = bf16[128,2048]{1,0:T(8,128)(2,1)} copy(bf16[128,2048]{1,0:T(8,128)(2,1)} %mixer_experts.1) | data formatting | bytes 1048576

commit v4 on v3

--- a/solution.py
+++ b/solution.py
@@ -78,12 +78,12 @@
     sp, tp = here.sp, here.tp
 
     barrier = pltpu.get_barrier_semaphore()
-    near = [here.at(0, 0, d // 2, d % 2) for d in range(1, 2 * SIDE)]
+    following = (sp + 1) % (DEVICES // 2)
+    previous = (sp + DEVICES // 2 - 1) % (DEVICES // 2)
+    near = [(sp, 1 - tp), (previous, tp), (previous, 1 - tp), (following, tp), (following, 1 - tp)]
+    near += [here.at(0, 0, d // 2, d % 2) for d in range(2, 2 * SIDE)]
     near += [here.at(0, d, 0, 0) for d in range(1, SIDE)]
     near += [here.at(d, 0, 0, 0) for d in range(1, SIDE)]
-    following = (sp + 1) % (DEVICES // 2)
-    previous = (sp + DEVICES // 2 - 1) % (DEVICES // 2)
-    near += [(following, 0), (following, 1), (previous, 0), (previous, 1)]
     for device in near:
         pl.semaphore_signal(barrier, inc=1, device_id=device, device_id_type=MESH)
 
@@ -102,8 +102,6 @@
     get_proj = fetch(7, proj_hbm, proj)
     ext[:REACH, :] = jnp.zeros((REACH, CHANNELS), BF16)
     pl.semaphore_wait(barrier, len(near))
-    for d in range(1, SIDE):
-        pl.semaphore_signal(plane_sem, inc=1, device_id=here.at(0, d, 0, 0), device_id_type=MESH)
     get_pool.wait()
 
     def slab(core):
@@ -123,6 +121,8 @@
     halos[0].start()
     halos[1].start()
     swap.start()
+    for d in range(1, SIDE):
+        pl.semaphore_signal(plane_sem, inc=1, device_id=here.at(0, d, 0, 0), device_id_type=MESH)
     get_sg = fetch(8, sg_hbm, sg)
     get_su = fetch(9, su_hbm, su)
     get_sd = fetch(10, sd_hbm, sd)
@@ -307,7 +307,7 @@
     return pl.pallas_call(
         kernel,
         name="mixer_experts",
-        out_shape=jax.ShapeDtypeStruct((TOKENS_HERE, D), BF16),
+        out_shape=pltpu.VMEM((TOKENS_HERE, D), BF16),
         in_specs=[any_space] * 14,
         out_specs=pl.BlockSpec(memory_space=pltpu.VMEM),
         scratch_shapes=[

time: 88 us -> 86.2 us (0.980)
  local copies, waits for them, and re-layouts: 1.88 us -> 0.8 us
    unnamed x1, local copies, waits for them, and re-layouts: 1.88 us -> 0.8 us
where the time goes in v4:
time: 86.2 us; the launch traced here: 86.1 us
  Pallas kernels  85.3 us (99%)
    pallas_call x1, Pallas kernels, on_device(): pl.pallas_call(kernel, name='mixer_experts', out_shape=pltpu.VMEM((TOKENS...  85.3 us

profile of v4, /device:TPU:1, one launch (start us, length us, event | category | flops | bytes accessed | tf_op | source)
XLA Modules:
  0.0 86.1 jit_solution(14527861146334735837)
XLA Ops:
  0.0 85.3 %mixer_experts.1 = bf16[128,2048]{1,0:T(8,128)(2,1)S(1)} custom-call(bf16[128,2048]{1,0:T(8,128)(2,1)} %res_hbm.1, bf16[256,512]{1,0:T(8,128)(2,1)} %pool_hbm.1, bf16[8,128,128]{2,1,0:T(8,128)(2,1)} %maps_hbm.1, f32[8,128]{1,0:T(8,128)} %bitcast.5, bf16[1024,2048]{1,0:T(8,128)(2,1)} %proj_hbm.1, f32[16,128]{1,0:T(8,128)} %bitcast.4, ...), custom_call_target="tpu_custom_call" | custom-call | tf_op jit(solution)/shard_map/mixer_experts/pallas_call | solution.py:307
  85.3 0.8 copy.16

commit v5 on v4

--- a/solution.py
+++ b/solution.py
@@ -28,22 +28,51 @@
 GROUPS = 4
 GW = 128
 REACH = 16
-STRIDE = 53
-PARTS = (16, 16, 32, 32, 16, 16)
-
-
-def members(part):
-    first = sum(PARTS[:part])
-    return range(max(first, 1), first + PARTS[part])
+STRIDE = 37
+ORDERS = 3
+COLUMNS = ((0, 640), (640, 640), (1280, 768))
+WIDEST = 768
+RINGS = 32 * SLOTS
+OFFSETS = (0, 1, 3, 2)
+WAVES = (1, 0)
+
+
+def boxes(a, dc):
+    every, others = pl.ds(0, SIDE), pl.ds(1, SIDE - 1)
+    if dc:
+        return [(every, every, every, 1)]
+    if a == 0:
+        return [(others, every, every, 0), (0, others, every, 0)]
+    if a == 1:
+        return [(others, every, every, 0), (0, every, others, 0)]
+    return [(every, others, every, 0), (every, 0, others, 0)]
+
+
+def back_boxes(dc):
+    every, others = pl.ds(0, SIDE), pl.ds(1, SIDE - 1)
+    if dc:
+        return [(every, every, every, 1)]
+    return [(others, every, every, 0), (0, others, every, 0), (0, 0, others, 0)]
+
+
+def box_id(a, dc, i):
+    return 3 * a + (2 if dc else i)
+
+
+def back_id(dc, i):
+    return 3 if dc else i
+
+
+def back_spots(dc):
+    for n in range(DEVICES // 2):
+        k = n * STRIDE % (DEVICES // 2)
+        spot = k // 16, k // 4 % SIDE, k % SIDE
+        if dc or any(spot):
+            yield spot, 0 if spot[0] else 1 if spot[1] else 2
 
 
 def dot(a, b):
     return jnp.dot(a, b, preferred_element_type=F32)
-
-
-def offset_of(k):
-    kk = k * STRIDE % DEVICES
-    return kk // 32, kk // 8 % SIDE, kk // 2 % SIDE, kk % 2
 
 
 class Place:
@@ -59,9 +88,11 @@
     def at(self, dz, dy, dx, dc):
         return self.z[dz % SIDE] + self.y[dy % SIDE] + self.x[dx % SIDE], self.c[dc]
 
-    def peer(self, k, sign):
-        dz, dy, dx, dc = offset_of(k)
-        return self.at(sign * dz, sign * dy, sign * dx, dc)
+    def along(self, a, d):
+        return self.at(*[(0, 0, d), (0, d, 0), (d, 0, 0)][a], 0)
+
+    def spot(self, p, u, v, dc, sign):
+        return self.at(sign * OFFSETS[p], sign * OFFSETS[u], sign * OFFSETS[v], dc)
 
 
 def kernel(
@@ -69,9 +100,11 @@
     sg_hbm, su_hbm, sd_hbm, eg_hbm, eu_hbm, ed_hbm, ids_hbm, score_hbm,
     out_ref,
     res, ext, maps, scale, proj, gain, sg, su, sd, eg, eu, ed, ids, score,
-    mix, other_ext, halo, settled, normed, acc, place, comb,
+    mix, other_ext, halo, settled, normed, acc,
+    ring_ids, place, comb, ring_rows,
     outgoing, arrived, results, returned,
     in_sems, halo_send, halo_recv, swap_send, swap_recv,
+    table_send, table_recv, ring_send, ring_recv, far_send, far_recv,
     out_send, out_recv, back_send, back_recv, plane_sem, cube_sem,
 ):
     here = Place()
@@ -132,34 +165,46 @@
 
     get_ids.wait()
     get_score.wait()
+    for a in range(ORDERS):
+        for j in range(1, SIDE):
+            pltpu.make_async_remote_copy(
+                ids, ring_ids.at[a, j], table_send, table_recv,
+                device_id=here.along(a, OFFSETS[j]), device_id_type=MESH,
+            ).start()
+
     expert = lax.broadcasted_iota(jnp.int32, (DEVICES, TOKENS_HERE), 0)
-    raw = score[...]
-    weights = raw / jnp.sum(raw, axis=0, keepdims=True) * routed_scale
-    chosen = jnp.zeros((DEVICES, TOKENS_HERE), F32)
-    weight = jnp.zeros((DEVICES, TOKENS_HERE), F32)
-    for k in range(TOPK):
-        hit = expert == ids[k : k + 1, :]
-        chosen = jnp.where(hit, 1.0, chosen)
-        weight = jnp.where(hit, weights[k : k + 1, :], weight)
-    row = lax.broadcasted_iota(jnp.int32, (TOKENS_HERE, TOKENS_HERE), 0)
-    column = lax.broadcasted_iota(jnp.int32, (TOKENS_HERE, TOKENS_HERE), 1)
-    earlier = (row < column).astype(BF16)
-    rank = dot(chosen.astype(BF16), earlier)
-    tag = chosen * (rank + 1.0)
-    slot_row = lax.broadcasted_iota(jnp.int32, (DEVICES * SLOTS, DEVICES), 0)
-    slot_expert = lax.broadcasted_iota(jnp.int32, (DEVICES * SLOTS, DEVICES), 1)
-    turn = (slot_row // SLOTS) * STRIDE % DEVICES
-    peer_z = (sp // 16 + turn // 32) % SIDE
-    peer_y = (sp // SIDE + turn // 8) % SIDE
-    peer_x = (sp + turn // 2) % SIDE
-    peer = ((peer_z * SIDE + peer_y) * SIDE + peer_x) * 2 + (tp + turn) % 2
-    spread = (peer == slot_expert).astype(BF16)
+    before = lax.broadcasted_iota(jnp.int32, (TOKENS_HERE, TOKENS_HERE), 0)
+    token = lax.broadcasted_iota(jnp.int32, (TOKENS_HERE, TOKENS_HERE), 1)
+    earlier = (before < token).astype(BF16)
+    slot_row = lax.broadcasted_iota(jnp.int32, (RINGS, DEVICES), 0)
+    slot_expert = lax.broadcasted_iota(jnp.int32, (RINGS, DEVICES), 1)
     slot_number = (slot_row % SLOTS + 1).astype(F32)
-    place[...] = (dot(spread, tag.astype(BF16)) == slot_number).astype(BF16)
-    weight_high = weight.astype(BF16)
-    weight_low = (weight - weight_high.astype(F32)).astype(BF16)
-    comb[:, :TOKENS_HERE] = dot(spread, weight_high).astype(BF16) * place[...]
-    comb[:, TOKENS_HERE:] = dot(spread, weight_low).astype(BF16) * place[...]
+    u, v, c = slot_row // 64, slot_row // 16 % SIDE, slot_row // 8 % 2
+    u, v = jnp.where(u < 2, u, 5 - u), jnp.where(v < 2, v, 5 - v)
+    z, y, x = sp // 16, sp // SIDE % SIDE, sp % SIDE
+    c = (tp + c) % 2
+
+    def spread_over(chip):
+        return (chip * 2 + c == slot_expert).astype(BF16)
+
+    spread = [
+        spread_over(((z + u) % SIDE * SIDE + (y + v) % SIDE) * SIDE + x),
+        spread_over(((z + u) % SIDE * SIDE + y) * SIDE + (x + v) % SIDE),
+        spread_over((z * SIDE + (y + u) % SIDE) * SIDE + (x + v) % SIDE),
+    ]
+
+    def tag_of(rows):
+        chosen = jnp.zeros((DEVICES, TOKENS_HERE), F32)
+        for k in range(TOPK):
+            chosen = jnp.where(expert == rows[k : k + 1, :], 1.0, chosen)
+        return (chosen * (dot(chosen.astype(BF16), earlier) + 1.0)).astype(BF16)
+
+    def set_place(a, j, tag):
+        place[a * SIDE + j] = (dot(spread[a], tag) == slot_number).astype(BF16)
+
+    own_tag = tag_of(ids[...])
+    for a in range(ORDERS):
+        set_place(a, 0, own_tag)
 
     pl.semaphore_wait(plane_sem, SIDE - 1)
     for d in range(1, SIDE):
@@ -216,27 +261,100 @@
         value = settled[:, lanes].astype(F32) * inverse * gain[j : j + 1, :]
         normed[:, lanes] = value.astype(BF16)
 
-    base = 0
-    for part, size in enumerate(PARTS):
-        for n in range(0, D, 512):
-            rows = dot(place[pl.ds(base * SLOTS, size * SLOTS), :], normed[:, n : n + 512])
-            outgoing[pl.ds(base, size), :, n : n + 512] = rows.astype(BF16).reshape(size, SLOTS, 512)
-        base += size
-        if part == 0:
-            pl.semaphore_wait(cube_sem, SIDE - 1)
-        for k in members(part):
-            pltpu.make_async_remote_copy(
-                outgoing.at[k, pl.ds(0, CAP)], arrived.at[k, pl.ds(0, CAP)],
-                out_send, out_recv.at[part],
-                device_id=here.peer(k, 1), device_id_type=MESH,
-            ).start()
-    arrived[0] = outgoing[0]
+    def ring(a, j):
+        first, width = COLUMNS[a]
+        return pltpu.make_async_remote_copy(
+            normed.at[:, pl.ds(first, width)], ring_rows.at[a, j, :, pl.ds(0, width)],
+            ring_send.at[a, j], ring_recv.at[a, j],
+            device_id=here.along(a, OFFSETS[j]), device_id_type=MESH,
+        )
+
+    def onward(a, j):
+        half = pl.ds((j - 1) * (TOKENS_HERE // 2), TOKENS_HERE // 2)
+        part = pl.ds(0, COLUMNS[a][1])
+        return pltpu.make_async_remote_copy(
+            ring_rows.at[a, j, half, part], ring_rows.at[a, 3, half, part],
+            far_send.at[a, j], far_recv.at[a, j],
+            device_id=here.along(a, OFFSETS[j]), device_id_type=MESH,
+        )
+
+    for j in (1, 2):
+        for a in range(ORDERS):
+            ring(a, j).start()
+
+    def block(ref, index, a):
+        first, width = COLUMNS[a]
+        return ref.at[(*index, pl.ds(0, CAP), pl.ds(first, width))]
+
+    def ship(dc, lead):
+        for u in range(SIDE):
+            for v in range(SIDE):
+                if u or v or dc:
+                    for a in range(ORDERS):
+                        spot = [(u, v, 0), (u, 0, v), (0, u, v)][a]
+                        index = [(u, v, lead), (u, lead, v), (lead, u, v)][a]
+                        sem = box_id(a, dc, 0 if u else 1)
+                        pltpu.make_async_remote_copy(
+                            block(outgoing, (*index, dc), a), block(arrived, (*index, dc), a),
+                            out_send.at[sem], out_recv.at[sem],
+                            device_id=here.spot(*spot, dc, 1), device_id_type=MESH,
+                        ).start()
+
+    def plane(a, j):
+        first, width = COLUMNS[a]
+        every, columns = slice(None), slice(first, first + width)
+        lead = [(every, every, j), (every, j, every), (j, every, every)][a]
+        return (*lead, every, every, columns)
+
+    def local(a):
+        first, width = COLUMNS[a]
+        every, columns = slice(None), slice(first, first + width)
+        lead = [(0, 0, every, 0), (0, every, 0, 0), (every, 0, 0, 0)][a]
+        return (*lead, every, columns)
+
+    def fill(a, j, rows):
+        value = dot(place[a * SIDE + j], rows).astype(BF16)
+        outgoing[plane(a, j)] = value.reshape(SIDE, SIDE, 2, SLOTS, COLUMNS[a][1])
+
+    for a, (first, width) in enumerate(COLUMNS):
+        fill(a, 0, normed[:, first : first + width])
+    pl.semaphore_wait(cube_sem, SIDE - 1)
+    for dc in WAVES:
+        ship(dc, 0)
+
+    others = pl.ds(1, SIDE - 1)
+    pltpu.make_async_remote_copy(
+        ring_ids.at[:, others], ring_ids.at[:, others], table_send, table_recv,
+        device_id=(sp, 1 - tp), device_id_type=MESH,
+    ).wait()
+    for a in range(ORDERS):
+        for j in (1, 2):
+            set_place(a, j, tag_of(ring_ids[a, j]))
+    for j in (1, 2):
+        for a in range(ORDERS):
+            ring(a, j).wait_recv()
+            onward(a, j).start()
+    for j in (1, 2):
+        for a in range(ORDERS):
+            fill(a, j, ring_rows[a, j, :, : COLUMNS[a][1]])
+    ship(WAVES[0], pl.ds(1, 2))
+    for a in range(ORDERS):
+        set_place(a, 3, tag_of(ring_ids[a, 3]))
+    for a in range(ORDERS):
+        onward(a, 1).wait_recv()
+        onward(a, 2).wait_recv()
+        fill(a, 3, ring_rows[a, 3, :, : COLUMNS[a][1]])
+    ship(WAVES[0], 3)
+    ship(WAVES[1], pl.ds(1, 2))
+    ship(WAVES[1], 3)
+    for a in range(ORDERS):
+        arrived[local(a)] = outgoing[local(a)]
 
     def clear(i, _):
-        returned[pl.ds(i * 8, 8), CAP:, :] = jnp.zeros((8, SLOTS - CAP, D), BF16)
+        returned[i // SIDE, i % SIDE, :, :, CAP:, :] = jnp.zeros((SIDE, 2, SLOTS - CAP, D), BF16)
         return 0
 
-    lax.fori_loop(0, DEVICES // 8, clear, 0)
+    lax.fori_loop(0, SIDE * SIDE, clear, 0)
 
     get_sg.wait()
     get_su.wait()
@@ -251,49 +369,80 @@
     get_eu.wait()
     get_ed.wait()
 
-    def span(src, dst, send_sem, recv_sem, first, count):
+    raw = score[...]
+    weights = raw / jnp.sum(raw, axis=0, keepdims=True) * routed_scale
+    weight = jnp.zeros((DEVICES, TOKENS_HERE), F32)
+    for k in range(TOPK):
+        weight = jnp.where(expert == ids[k : k + 1, :], weights[k : k + 1, :], weight)
+    high = weight.astype(BF16)
+    low = (weight - high.astype(F32)).astype(BF16)
+    slot_row = lax.broadcasted_iota(jnp.int32, (2 * RINGS, DEVICES), 0)
+    slot_expert = lax.broadcasted_iota(jnp.int32, (2 * RINGS, DEVICES), 1)
+    slot_number = (slot_row % SLOTS + 1).astype(F32)
+    w, u, v = slot_row // 128, slot_row // 32 % SIDE, slot_row // 8 % SIDE
+    w, u, v = [jnp.where(i < 2, i, 5 - i) for i in (w, u, v)]
+    chip = ((z + w) % SIDE * SIDE + (y + u) % SIDE) * SIDE + (x + v) % SIDE
+    for dc in range(2):
+        over = (chip * 2 + (tp + dc) % 2 == slot_expert).astype(BF16)
+        where = (dot(over, own_tag) == slot_number).astype(F32)
+        comb[dc, :TOKENS_HERE, :] = (dot(over, high) * where).T.astype(BF16)
+        comb[dc, TOKENS_HERE:, :] = (dot(over, low) * where).T.astype(BF16)
+
+    def box(a, dc, i):
+        index, sem = boxes(a, dc)[i], box_id(a, dc, i)
         return pltpu.make_async_remote_copy(
-            src.at[pl.ds(first, count), pl.ds(0, CAP)], dst.at[pl.ds(first, count), pl.ds(0, CAP)],
-            send_sem, recv_sem, device_id=(sp, 1 - tp), device_id_type=MESH,
+            block(outgoing, index, a), block(arrived, index, a), out_send.at[sem], out_recv.at[sem],
+            device_id=(sp, 1 - tp), device_id_type=MESH,
         )
 
-    base = 0
-    for part, size in enumerate(PARTS):
-        ks = members(part)
-        span(outgoing, arrived, out_send, out_recv.at[part], ks[0], len(ks)).wait_recv()
-        rows = arrived[pl.ds(base, size)].reshape(size * SLOTS, D)
-        hidden = dot(rows, eg[...])
-        hidden = hidden / (1.0 + jnp.exp(-hidden)) * dot(rows, eu[...])
-        hidden = hidden.astype(BF16)
+    def back_copy(index, sem, device):
+        index = (*index, pl.ds(0, CAP))
+        return pltpu.make_async_remote_copy(
+            results.at[index], returned.at[index], back_send.at[sem], back_recv.at[sem],
+            device_id=device, device_id_type=MESH,
+        )
+
+    def back_box(dc, i):
+        return back_copy(back_boxes(dc)[i], back_id(dc, i), (sp, 1 - tp))
+
+    for dc in WAVES:
+        for a in range(ORDERS):
+            for i in range(len(boxes(a, dc))):
+                box(a, dc, i).wait_recv()
+        for p in range(0, SIDE, 2):
+            rows = arrived[p : p + 2, :, :, dc].reshape(RINGS, D)
+            hidden = dot(rows, eg[...])
+            hidden = hidden / (1.0 + jnp.exp(-hidden)) * dot(rows, eu[...])
+            hidden = hidden.astype(BF16)
+            for n in range(0, D, 512):
+                value = dot(hidden, ed[:, n : n + 512]).astype(BF16)
+                results[p : p + 2, :, :, dc, :, n : n + 512] = value.reshape(2, SIDE, SIDE, SLOTS, 512)
+        for spot, i in back_spots(dc):
+            back_copy((*spot, dc), back_id(dc, i), here.spot(*spot, dc, -1)).start()
+    returned[0, 0, 0, 0] = results[0, 0, 0, 0]
+
+    for dc in WAVES:
+        for i in range(len(back_boxes(dc))):
+            back_box(dc, i).wait_recv()
         for n in range(0, D, 512):
-            value = dot(hidden, ed[:, n : n + 512]).astype(BF16)
-            results[pl.ds(base, size), :, n : n + 512] = value.reshape(size, SLOTS, 512)
-        for k in ks:
-            pltpu.make_async_remote_copy(
-                results.at[k, pl.ds(0, CAP)], returned.at[k, pl.ds(0, CAP)],
-                back_send, back_recv.at[part],
-                device_id=here.peer(k, -1), device_id_type=MESH,
-            ).start()
-        base += size
-    returned[0] = results[0]
-
-    base = 0
-    for part, size in enumerate(PARTS):
-        ks = members(part)
-        span(results, returned, back_send, back_recv.at[part], ks[0], len(ks)).wait_recv()
-        factors = comb[pl.ds(base * SLOTS, size * SLOTS), :].T
-        for n in range(0, D, 512):
-            rows = returned[pl.ds(base, size), :, n : n + 512].reshape(size * SLOTS, 512)
-            both = dot(factors, rows)
+            rows = returned[:, :, :, dc, :, n : n + 512].reshape(2 * RINGS, 512)
+            both = dot(comb[dc], rows)
             value = acc[:, n : n + 512] + (both[:TOKENS_HERE] + both[TOKENS_HERE:])
-            if part < len(PARTS) - 1:
+            if dc != WAVES[-1]:
                 acc[:, n : n + 512] = value
             else:
                 out_ref[:, n : n + 512] = value.astype(BF16)
-        base += size
-
-    span(outgoing, arrived, out_send, out_recv.at[0], 1, DEVICES - 1).wait_send()
-    span(results, returned, back_send, back_recv.at[0], 1, DEVICES - 1).wait_send()
+
+    for dc in range(2):
+        for a in range(ORDERS):
+            for i in range(len(boxes(a, dc))):
+                box(a, dc, i).wait_send()
+        for i in range(len(back_boxes(dc))):
+            back_box(dc, i).wait_send()
+    for a in range(ORDERS):
+        for j in (1, 2):
+            ring(a, j).wait_send()
+            onward(a, j).wait_send()
 
 
 def on_device(
@@ -303,7 +452,8 @@
 ):
     any_space = pl.BlockSpec(memory_space=pl.ANY)
     vmem = pltpu.VMEM
-    block = (DEVICES, SLOTS, D)
+    block = (SIDE, SIDE, SIDE, 2, SLOTS, D)
+    dma = pltpu.SemaphoreType.DMA
     return pl.pallas_call(
         kernel,
         name="mixer_experts",
@@ -331,21 +481,18 @@
             vmem((TOKENS_HERE, D), BF16),
             vmem((TOKENS_HERE, D), BF16),
             vmem((TOKENS_HERE, D), F32),
-            vmem((DEVICES * SLOTS, TOKENS_HERE), BF16),
-            vmem((DEVICES * SLOTS, 2 * TOKENS_HERE), BF16),
+            vmem((ORDERS, SIDE, TOPK, TOKENS_HERE), jnp.int32),
+            vmem((ORDERS * SIDE, RINGS, TOKENS_HERE), BF16),
+            vmem((2, 2 * TOKENS_HERE, 2 * RINGS), BF16),
+            vmem((ORDERS, SIDE, TOKENS_HERE, WIDEST), BF16),
             vmem(block, BF16),
             vmem(block, BF16),
             vmem(block, BF16),
             vmem(block, BF16),
-            pltpu.SemaphoreType.DMA((14,)),
-            pltpu.SemaphoreType.DMA((2,)),
-            pltpu.SemaphoreType.DMA((2,)),
-            pltpu.SemaphoreType.DMA,
-            pltpu.SemaphoreType.DMA,
-            pltpu.SemaphoreType.DMA,
-            pltpu.SemaphoreType.DMA((len(PARTS),)),
-            pltpu.SemaphoreType.DMA,
-            pltpu.SemaphoreType.DMA((len(PARTS),)),
+            dma((14,)),
+            dma((2,)), dma((2,)), dma, dma,
+            dma, dma, dma((ORDERS, SIDE)), dma((ORDERS, SIDE)), dma((ORDERS, SIDE)), dma((ORDERS, SIDE)),
+            dma((9,)), dma((9,)), dma((4,)), dma((4,)),
             pltpu.SemaphoreType.REGULAR,
             pltpu.SemaphoreType.REGULAR,
         ],

time: 86.2 us -> 81.7 us (0.948)
  Pallas kernels: 85.3 us -> 80.8 us
    pallas_call x1, Pallas kernels: 85.3 us -> 80.8 us  [on_device(): pl.pallas_call(kernel, name='mixer_experts', out_shape=pltpu.VMEM((TOKENS...]
where the time goes in v5:
time: 81.7 us; the launch traced here: 81.6 us
  Pallas kernels  80.8 us (99%)
    pallas_call x1, Pallas kernels, on_device(): pl.pallas_call(kernel, name='mixer_experts', out_shape=pltpu.VMEM((TOKENS...  80.8 us

profile of v5, /device:TPU:1, one launch (start us, length us, event | category | flops | bytes accessed | tf_op | source)
XLA Modules:
  0.0 81.6 jit_solution(11444705317968352694)
XLA Ops:
  0.0 80.8 %mixer_experts.1 = bf16[128,2048]{1,0:T(8,128)(2,1)S(1)} custom-call(bf16[128,2048]{1,0:T(8,128)(2,1)} %res_hbm.1, bf16[256,512]{1,0:T(8,128)(2,1)} %pool_hbm.1, bf16[8,128,128]{2,1,0:T(8,128)(2,1)} %maps_hbm.1, f32[8,128]{1,0:T(8,128)} %bitcast.5, bf16[1024,2048]{1,0:T(8,128)(2,1)} %proj_hbm.1, f32[16,128]{1,0:T(8,128)} %bitcast.4, ...), custom_call_target="tpu_custom_call" | custom-call | tf_op jit(solution)/shard_map/mixer_experts/pallas_call | solution.py:457
  80.8 0.8 copy.16

commit v6 on v5

--- a/solution.py
+++ b/solution.py
@@ -34,6 +34,7 @@
 WIDEST = 768
 RINGS = 32 * SLOTS
 OFFSETS = (0, 1, 3, 2)
+HALVES = (1, 0)
 WAVES = (1, 0)
 
 
@@ -48,27 +49,27 @@
     return [(every, others, every, 0), (every, 0, others, 0)]
 
 
-def back_boxes(dc):
-    every, others = pl.ds(0, SIDE), pl.ds(1, SIDE - 1)
-    if dc:
-        return [(every, every, every, 1)]
-    return [(others, every, every, 0), (0, others, every, 0), (0, 0, others, 0)]
+def back_boxes(dc, half):
+    every, others, both = pl.ds(0, SIDE), pl.ds(1, SIDE - 1), pl.ds(2 * half, 2)
+    if dc or half:
+        return [(every, every, both, dc)]
+    return [(others, every, both, 0), (0, others, both, 0), (0, 0, 1, 0)]
 
 
 def box_id(a, dc, i):
     return 3 * a + (2 if dc else i)
 
 
-def back_id(dc, i):
-    return 3 if dc else i
-
-
-def back_spots(dc):
+def back_id(dc, half, i):
+    return 2 + half if dc else 4 if half else i if i < 2 else 5
+
+
+def back_spots(dc, half):
     for n in range(DEVICES // 2):
         k = n * STRIDE % (DEVICES // 2)
         spot = k // 16, k // 4 % SIDE, k % SIDE
-        if dc or any(spot):
-            yield spot, 0 if spot[0] else 1 if spot[1] else 2
+        if spot[2] // 2 == half and (dc or any(spot)):
+            yield spot, 0 if dc or half or spot[0] else 1 if spot[1] else 2
 
 
 def dot(a, b):
@@ -356,37 +357,38 @@
 
     lax.fori_loop(0, SIDE * SIDE, clear, 0)
 
-    get_sg.wait()
-    get_su.wait()
-    get_sd.wait()
-    hidden = dot(normed[...], sg[...])
-    hidden = hidden / (1.0 + jnp.exp(-hidden)) * dot(normed[...], su[...])
-    hidden = hidden.astype(BF16)
-    for n in range(0, D, 512):
-        acc[:, n : n + 512] = settled[:, n : n + 512].astype(F32) + dot(hidden, sd[:, n : n + 512])
-
     get_eg.wait()
     get_eu.wait()
     get_ed.wait()
 
-    raw = score[...]
-    weights = raw / jnp.sum(raw, axis=0, keepdims=True) * routed_scale
-    weight = jnp.zeros((DEVICES, TOKENS_HERE), F32)
-    for k in range(TOPK):
-        weight = jnp.where(expert == ids[k : k + 1, :], weights[k : k + 1, :], weight)
-    high = weight.astype(BF16)
-    low = (weight - high.astype(F32)).astype(BF16)
-    slot_row = lax.broadcasted_iota(jnp.int32, (2 * RINGS, DEVICES), 0)
-    slot_expert = lax.broadcasted_iota(jnp.int32, (2 * RINGS, DEVICES), 1)
-    slot_number = (slot_row % SLOTS + 1).astype(F32)
-    w, u, v = slot_row // 128, slot_row // 32 % SIDE, slot_row // 8 % SIDE
-    w, u, v = [jnp.where(i < 2, i, 5 - i) for i in (w, u, v)]
-    chip = ((z + w) % SIDE * SIDE + (y + u) % SIDE) * SIDE + (x + v) % SIDE
-    for dc in range(2):
-        over = (chip * 2 + (tp + dc) % 2 == slot_expert).astype(BF16)
-        where = (dot(over, own_tag) == slot_number).astype(F32)
-        comb[dc, :TOKENS_HERE, :] = (dot(over, high) * where).T.astype(BF16)
-        comb[dc, TOKENS_HERE:, :] = (dot(over, low) * where).T.astype(BF16)
+    def beside():
+        get_sg.wait()
+        get_su.wait()
+        get_sd.wait()
+        hidden = dot(normed[...], sg[...])
+        hidden = hidden / (1.0 + jnp.exp(-hidden)) * dot(normed[...], su[...])
+        hidden = hidden.astype(BF16)
+        for n in range(0, D, 512):
+            acc[:, n : n + 512] = settled[:, n : n + 512].astype(F32) + dot(hidden, sd[:, n : n + 512])
+
+
+        raw = score[...]
+        weights = raw / jnp.sum(raw, axis=0, keepdims=True) * routed_scale
+        weight = jnp.zeros((DEVICES, TOKENS_HERE), F32)
+        for k in range(TOPK):
+            weight = jnp.where(expert == ids[k : k + 1, :], weights[k : k + 1, :], weight)
+        high = weight.astype(BF16)
+        low = (weight - high.astype(F32)).astype(BF16)
+        w, u, v = slot_row // 64, slot_row // 16 % SIDE, slot_row // 8 % 2
+        w, u = [jnp.where(i < 2, i, 5 - i) for i in (w, u)]
+        for dc in range(2):
+            for half in range(2):
+                along = 3 - v if half else v
+                chip = ((z + w) % SIDE * SIDE + (y + u) % SIDE) * SIDE + (x + along) % SIDE
+                over = (chip * 2 + (tp + dc) % 2 == slot_expert).astype(BF16)
+                where = (dot(over, own_tag) == slot_number).astype(F32)
+                comb[2 * dc + half, :TOKENS_HERE, :] = (dot(over, high) * where).T.astype(BF16)
+                comb[2 * dc + half, TOKENS_HERE:, :] = (dot(over, low) * where).T.astype(BF16)
 
     def box(a, dc, i):
         index, sem = boxes(a, dc)[i], box_id(a, dc, i)
@@ -402,43 +404,49 @@
             device_id=device, device_id_type=MESH,
         )
 
-    def back_box(dc, i):
-        return back_copy(back_boxes(dc)[i], back_id(dc, i), (sp, 1 - tp))
+    def back_box(dc, half, i):
+        index = back_boxes(dc, half)[i]
+        return back_copy(index, back_id(dc, half, i), (sp, 1 - tp))
 
     for dc in WAVES:
         for a in range(ORDERS):
             for i in range(len(boxes(a, dc))):
                 box(a, dc, i).wait_recv()
-        for p in range(0, SIDE, 2):
-            rows = arrived[p : p + 2, :, :, dc].reshape(RINGS, D)
+        for half in HALVES:
+            xs = slice(2 * half, 2 * half + 2)
+            rows = arrived[:, :, xs, dc].reshape(RINGS, D)
             hidden = dot(rows, eg[...])
             hidden = hidden / (1.0 + jnp.exp(-hidden)) * dot(rows, eu[...])
             hidden = hidden.astype(BF16)
             for n in range(0, D, 512):
                 value = dot(hidden, ed[:, n : n + 512]).astype(BF16)
-                results[p : p + 2, :, :, dc, :, n : n + 512] = value.reshape(2, SIDE, SIDE, SLOTS, 512)
-        for spot, i in back_spots(dc):
-            back_copy((*spot, dc), back_id(dc, i), here.spot(*spot, dc, -1)).start()
+                results[:, :, xs, dc, :, n : n + 512] = value.reshape(SIDE, SIDE, 2, SLOTS, 512)
+            for spot, i in back_spots(dc, half):
+                back_copy((*spot, dc), back_id(dc, half, i), here.spot(*spot, dc, -1)).start()
+        if dc == WAVES[0]:
+            beside()
     returned[0, 0, 0, 0] = results[0, 0, 0, 0]
 
     for dc in WAVES:
-        for i in range(len(back_boxes(dc))):
-            back_box(dc, i).wait_recv()
-        for n in range(0, D, 512):
-            rows = returned[:, :, :, dc, :, n : n + 512].reshape(2 * RINGS, 512)
-            both = dot(comb[dc], rows)
-            value = acc[:, n : n + 512] + (both[:TOKENS_HERE] + both[TOKENS_HERE:])
-            if dc != WAVES[-1]:
-                acc[:, n : n + 512] = value
-            else:
-                out_ref[:, n : n + 512] = value.astype(BF16)
+        for half in HALVES:
+            for i in range(len(back_boxes(dc, half))):
+                back_box(dc, half, i).wait_recv()
+            for n in range(0, D, 512):
+                rows = returned[:, :, 2 * half : 2 * half + 2, dc, :, n : n + 512]
+                both = dot(comb[2 * dc + half], rows.reshape(RINGS, 512))
+                value = acc[:, n : n + 512] + (both[:TOKENS_HERE] + both[TOKENS_HERE:])
+                if dc != WAVES[-1] or half != HALVES[-1]:
+                    acc[:, n : n + 512] = value
+                else:
+                    out_ref[:, n : n + 512] = value.astype(BF16)
 
     for dc in range(2):
         for a in range(ORDERS):
             for i in range(len(boxes(a, dc))):
                 box(a, dc, i).wait_send()
-        for i in range(len(back_boxes(dc))):
-            back_box(dc, i).wait_send()
+        for half in range(2):
+            for i in range(len(back_boxes(dc, half))):
+                back_box(dc, half, i).wait_send()
     for a in range(ORDERS):
         for j in (1, 2):
             ring(a, j).wait_send()
@@ -483,7 +491,7 @@
             vmem((TOKENS_HERE, D), F32),
             vmem((ORDERS, SIDE, TOPK, TOKENS_HERE), jnp.int32),
             vmem((ORDERS * SIDE, RINGS, TOKENS_HERE), BF16),
-            vmem((2, 2 * TOKENS_HERE, 2 * RINGS), BF16),
+            vmem((4, 2 * TOKENS_HERE, RINGS), BF16),
             vmem((ORDERS, SIDE, TOKENS_HERE, WIDEST), BF16),
             vmem(block, BF16),
             vmem(block, BF16),
@@ -492,7 +500,7 @@
             dma((14,)),
             dma((2,)), dma((2,)), dma, dma,
             dma, dma, dma((ORDERS, SIDE)), dma((ORDERS, SIDE)), dma((ORDERS, SIDE)), dma((ORDERS, SIDE)),
-            dma((9,)), dma((9,)), dma((4,)), dma((4,)),
+            dma((9,)), dma((9,)), dma((6,)), dma((6,)),
             pltpu.SemaphoreType.REGULAR,
             pltpu.SemaphoreType.REGULAR,
         ],

time: 81.7 us -> 81.4 us (level)
  no operation moved by 1% of the time
where the time goes in v6:
time: 81.4 us; the launch traced here: 81.3 us
  Pallas kernels  80.5 us (99%)
    pallas_call x1, Pallas kernels, on_device(): pl.pallas_call(kernel, name='mixer_experts', out_shape=pltpu.VMEM((TOKENS...  80.5 us

profile of v6, /device:TPU:1, one launch (start us, length us, event | category | flops | bytes accessed | tf_op | source)
XLA Modules:
  0.0 81.3 jit_solution(682423064558241678)
XLA Ops:
  0.0 80.5 %mixer_experts.1 = bf16[128,2048]{1,0:T(8,128)(2,1)S(1)} custom-call(bf16[128,2048]{1,0:T(8,128)(2,1)} %res_hbm.1, bf16[256,512]{1,0:T(8,128)(2,1)} %pool_hbm.1, bf16[8,128,128]{2,1,0:T(8,128)(2,1)} %maps_hbm.1, f32[8,128]{1,0:T(8,128)} %bitcast.5, bf16[1024,2048]{1,0:T(8,128)(2,1)} %proj_hbm.1, f32[16,128]{1,0:T(8,128)} %bitcast.4, ...), custom_call_target="tpu_custom_call" | custom-call | tf_op jit(solution)/shard_map/mixer_experts/pallas_call | solution.py:465
  80.5 0.8 copy.16
